TPU v7x, 32 devices: a whole 2x2x4 slice. The times are simulated.
32 devices in a mesh: sp: 16 (over z, y, core), tp: 2 (over x).
Axes of the slice: x: 2, y: 2, z: 4, core: 2. Of those that a mesh axis runs over, the one named last changes fastest.
Arguments:
- residual: bfloat16 [2048, 2048], P(('sp', 'tp')), may hold values from -6 to 6
- forget_forward: bfloat16 [2048, 1024], P('sp', 'tp'), may hold values from -5.5 to 5.5
- forget_backward: bfloat16 [2048, 1024], P('sp', 'tp'), may hold values from -5.5 to 5.5
- value_written: bfloat16 [2048, 1024], P('sp', 'tp'), may hold values from -6 to 6
- query_logits: bfloat16 [2048, 1024], P('sp', 'tp'), may hold values from -6 to 6
- output_gate_logits: bfloat16 [2048, 1024], P('sp', 'tp'), may hold values from -6 to 6
- forget_minimum: float32 [2, 1024], P(None, 'tp'), may hold values from 0.88 to 1
- extra_log_rate: float32 [2, 2048, 8], P(None, 'sp', 'tp'), may hold values from -0.7 to 0
- head_norm_scale: float32 [128], replicated, may hold values from 0.1 to 1.9
- output_matrix: bfloat16 [1024, 2048], P(None, 'sp'), may hold values from -0.1875 to 0.1875
- prenorm_scale: float32 [2048], replicated, may hold values from 0.1 to 1.9
- gate_up_matrix: bfloat16 [2048, 5632], P('sp', 'tp'), may hold values from -0.125 to 0.125
- value_up_matrix: bfloat16 [2048, 5632], P('sp', 'tp'), may hold values from -0.125 to 0.125
- gate_taps: float32 [3, 5632], P(None, 'tp'), may hold values from -3.5 to 3.5
- value_taps: float32 [3, 5632], P(None, 'tp'), may hold values from -3.5 to 3.5
- down_matrix: bfloat16 [5632, 2048], P('tp', 'sp'), may hold values from -0.078125 to 0.078125
Outputs:
- layer_out: bfloat16 [2048, 2048], P(('sp', 'tp'))
All inputs are finite; a program needn't handle non-finite values.
Results may differ from a plain program's by a relative error of at most 0.012.
Values may be sent and summed in bfloat16 or wider, within the bound.
A program may use at most 128 MiB of HBM per device.

v0:
```python
import functools
import math

import jax
import jax.numpy as jnp
from jax import lax
from jax.experimental import pallas as pl
from jax.experimental.pallas import tpu as pltpu
from jax.sharding import PartitionSpec as P

HEAD_WIDTH = 128
EPSILON = 1e-06
MESH = pl.DeviceIdType.MESH
F32 = jnp.float32
BF16 = jnp.bfloat16
DECAY_ROWS = 16
CHUNKS = 4


class Grid:
    def __init__(self, mesh):
        sp, tp = mesh.shape["sp"], mesh.shape["tp"]
        self.sp, self.x = sp, tp
        self.c = math.gcd(sp, 2)
        self.y = math.gcd(sp // self.c, 2)
        self.z = sp // (self.c * self.y)
        self.ids = iter(range(100))

    def size(self, dim):
        return getattr(self, dim)

    def place(self):
        s, t = lax.axis_index("sp"), lax.axis_index("tp")
        return {
            "sp": s,
            "x": t,
            "c": lax.rem(s, self.c),
            "y": lax.rem(s // self.c, self.y),
            "z": s // (self.c * self.y),
        }

    def peer(self, place, dim, index):
        if dim == "sp":
            return {"sp": index, "tp": place["x"]}
        at = dict(place)
        at[dim] = index
        return {"sp": (at["z"] * self.y + at["y"]) * self.c + at["c"], "tp": at["x"]}

    def greet(self, place, dims):
        barrier = pltpu.get_barrier_semaphore()
        count = 0
        for dim in dims:
            n = self.size(dim)
            for k in range(1, n):
                peer = self.peer(place, dim, lax.rem(place[dim] + k, n))
                pl.semaphore_signal(barrier, inc=1, device_id=peer, device_id_type=MESH)
                count += 1
        pl.semaphore_wait(barrier, count)


def exchange_kernel(grid, dims, keep, *refs):
    m = len(dims)
    ins, outs = refs[:m], refs[m : 2 * m]
    send_sem, recv_sem, own_sem = refs[2 * m :]
    place = grid.place()
    copies = []
    grid.greet(place, sorted(set(dims)))
    base = 0
    for i, dim in enumerate(dims):
        n, me = grid.size(dim), place[dim]
        for k in range(1, n):
            to = lax.rem(me + k, n)
            slot = me if keep else k - 1
            copy = pltpu.make_async_remote_copy(
                src_ref=ins[i].at[to],
                dst_ref=outs[i].at[slot],
                send_sem=send_sem.at[base + k - 1],
                recv_sem=recv_sem.at[base + k - 1],
                device_id=grid.peer(place, dim, to),
                device_id_type=MESH,
            )
            copy.start()
            copies.append(copy)
        base += n - 1
    if keep:
        for i, dim in enumerate(dims):
            me = place[dim]
            own = pltpu.make_async_copy(ins[i].at[me], outs[i].at[me], own_sem.at[i])
            own.start()
            copies.append(own)
    for copy in copies:
        copy.wait()


def exchange(grid, items, keep):
    dims = tuple(d for _, d in items)
    total = sum(grid.size(d) - 1 for d in dims)
    shapes = tuple(
        jax.ShapeDtypeStruct(a.shape if keep else (a.shape[0] - 1,) + a.shape[1:], a.dtype)
        for a, _ in items
    )
    return pl.pallas_call(
        functools.partial(exchange_kernel, grid, dims, keep),
        out_shape=shapes,
        in_specs=[pl.BlockSpec(memory_space=pl.ANY)] * len(items),
        out_specs=[pl.BlockSpec(memory_space=pl.ANY)] * len(items),
        scratch_shapes=[
            pltpu.SemaphoreType.DMA((total,)),
            pltpu.SemaphoreType.DMA((total,)),
            pltpu.SemaphoreType.DMA((len(items),)),
        ],
        compiler_params=pltpu.CompilerParams(
            collective_id=next(grid.ids), has_side_effects=True
        ),
    )(*[a for a, _ in items])


def gather_kernel(grid, x_ref, out_ref, send_sem, recv_sem, own_sem):
    place = grid.place()
    z, y, c, x = (place[d] for d in "zycx")
    part = x_ref.shape[1] // (2 * CHUNKS)
    grid.greet(place, ("z", "y", "c", "x"))
    own = pltpu.make_async_copy(x_ref, out_ref.at[z, y, c, x], own_sem)
    own.start()
    used = 0

    def push(dim, src, dst):
        nonlocal used
        n, copies = grid.size(dim), []
        for k in range(1, n):
            copy = pltpu.make_async_remote_copy(
                src_ref=src,
                dst_ref=dst,
                send_sem=send_sem.at[used],
                recv_sem=recv_sem.at[used],
                device_id=grid.peer(place, dim, lax.rem(place[dim] + k, n)),
                device_id_type=MESH,
            )
            copy.start()
            copies.append(copy)
            used += 1
        return copies

    def start(level, t):
        both = pl.ds(2 * t * part, 2 * part)
        first, second = pl.ds(2 * t * part, part), pl.ds((2 * t + 1) * part, part)
        if level == 0:
            return push("z", x_ref.at[:, both], out_ref.at[z, y, c, x, :, both])
        if level == 1:
            a = out_ref.at[:, y, c, x, :, first]
            b = out_ref.at[:, y, c, x, :, second]
            return push("y", a, a) + push("x", b, b)
        if level == 2:
            a = out_ref.at[:, :, c, x, :, first]
            b = out_ref.at[:, y, c, :, :, second]
            return push("x", a, a) + push("y", b, b)
        a = out_ref.at[:, :, c, :, :, both]
        return push("c", a, a)

    flying = {(0, t): start(0, t) for t in range(CHUNKS)}
    own.wait()
    for step in range(CHUNKS + 3):
        for level in range(4):
            t = step - level
            if 0 <= t < CHUNKS:
                for copy in flying[level, t]:
                    copy.wait()
                if level < 3:
                    flying[level + 1, t] = start(level + 1, t)


def gather(grid, array):
    total = CHUNKS * sum(grid.size(d) - 1 for d in "zyyxxc")
    return pl.pallas_call(
        functools.partial(gather_kernel, grid),
        out_shape=jax.ShapeDtypeStruct(
            (grid.z, grid.y, grid.c, grid.x) + array.shape, array.dtype
        ),
        in_specs=[pl.BlockSpec(memory_space=pltpu.VMEM)],
        out_specs=pl.BlockSpec(memory_space=pl.ANY),
        scratch_shapes=[
            pltpu.SemaphoreType.DMA((total,)),
            pltpu.SemaphoreType.DMA((total,)),
            pltpu.SemaphoreType.DMA,
        ],
        compiler_params=pltpu.CompilerParams(
            collective_id=next(grid.ids), has_side_effects=True
        ),
    )(array)


ORDERS = ("cxyz", "cyxz")


def reduce_kernel(grid, a_ref, b_ref, out_ref, *scratch):
    held, got, (send_sem, recv_sem, own_sem) = scratch[:2], scratch[2:10], scratch[10:]
    terms = (a_ref, b_ref)
    place = grid.place()
    rows, part = held[0].shape[-2:]
    grid.greet(place, ("z", "y", "c", "x"))
    used = 0

    def start(level, t):
        nonlocal used
        copies = []
        for color in range(2):
            dim = ORDERS[color][level]
            n, me = grid.size(dim), place[dim]
            for k in range(1, n):
                to = lax.rem(me + k, n)
                if level == 0:
                    src = terms[color].at[to, :, :, :, :, pl.ds(t * part, part)]
                else:
                    before = tuple(place[d] for d in ORDERS[color][1:level])
                    src = held[color].at[(t,) + before + (to,)]
                copy = pltpu.make_async_remote_copy(
                    src_ref=src,
                    dst_ref=got[2 * level + color].at[t, k - 1],
                    send_sem=send_sem.at[used],
                    recv_sem=recv_sem.at[used],
                    device_id=grid.peer(place, dim, to),
                    device_id_type=MESH,
                )
                copy.start()
                copies.append(copy)
                used += 1
        return copies

    def add(level, t):
        for color in range(2):
            order = ORDERS[color]
            here = tuple(place[d] for d in order[1 : level + 1])
            left = [grid.size(d) for d in order[level + 1 :]]
            peers = grid.size(order[level]) - 1
            where = got[2 * level + color]

            def block(i, _, color=color, here=here, left=left, peers=peers, where=where):
                index, rest = [], i
                for n in reversed(left):
                    index.insert(0, lax.rem(rest, n))
                    rest = rest // n
                index = tuple(index)
                total = held[color][(t,) + here + index].astype(F32)
                for k in range(peers):
                    total += where[(t, k) + index].astype(F32)
                if level < 3:
                    held[color][(t,) + here + index] = total.astype(BF16)
                else:
                    first = (color * CHUNKS + t) * part
                    out_ref[:, first : first + part] = total
                return 0

            if left:
                lax.fori_loop(0, math.prod(left), block, 0)
            else:
                block(0, 0)

    flying = {(0, t): start(0, t) for t in range(CHUNKS)}
    for t in range(CHUNKS):
        for color in range(2):
            own = pltpu.make_async_copy(
                terms[color].at[place["c"], :, :, :, :, pl.ds(t * part, part)],
                held[color].at[t],
                own_sem.at[t, color],
            )
            own.start()
            flying[0, t].append(own)
    for step in range(CHUNKS + 3):
        for level in range(4):
            t = step - level
            if 0 <= t < CHUNKS:
                for copy in flying[level, t]:
                    copy.wait()
                add(level, t)
                if level < 3:
                    flying[level + 1, t] = start(level + 1, t)


def reduce_scatter(grid, first, second):
    rows, cols = first.shape[-2:]
    tile = (rows, cols // CHUNKS)

    def sizes(order):
        return tuple(grid.size(d) for d in order)

    scratch = [pltpu.VMEM((CHUNKS,) + sizes(o[1:]) + tile, BF16) for o in ORDERS]
    for level in range(4):
        for o in ORDERS:
            peers = grid.size(o[level]) - 1
            scratch.append(
                pltpu.VMEM((CHUNKS, max(peers, 1)) + sizes(o[level + 1 :]) + tile, BF16)
            )
    total = 2 * CHUNKS * sum(grid.size(d) - 1 for d in "cxyz")
    return pl.pallas_call(
        functools.partial(reduce_kernel, grid),
        out_shape=jax.ShapeDtypeStruct((rows, 2 * cols), F32),
        in_specs=[pl.BlockSpec(memory_space=pl.ANY)] * 2,
        out_specs=pl.BlockSpec(memory_space=pltpu.VMEM),
        scratch_shapes=scratch
        + [
            pltpu.SemaphoreType.DMA((total,)),
            pltpu.SemaphoreType.DMA((total,)),
            pltpu.SemaphoreType.DMA((CHUNKS, 2)),
        ],
        compiler_params=pltpu.CompilerParams(
            collective_id=next(grid.ids), has_side_effects=True, vmem_limit_bytes=64000000
        ),
    )(first, second)


def dot(a, b, dims, precision=None):
    return lax.dot_general(
        a, b, (dims, ((), ())), precision=precision, preferred_element_type=F32
    )


def local_kernel(
    heads, zf_ref, zb_ref, v_ref, q_ref, floor_ref, extra_ref, out_ref, carry_ref, state_ref, decay_ref
):
    length = v_ref.shape[0]
    rows = lax.broadcasted_iota(jnp.int32, (length, length), 0)
    cols = lax.broadcasted_iota(jnp.int32, (length, length), 1)
    middle = length // 2
    for h in range(heads):
        at = slice(h * HEAD_WIDTH, (h + 1) * HEAD_WIDTH)
        values = v_ref[:, at]
        logits = q_ref[:, at].astype(F32)
        queries = logits * jax.nn.sigmoid(logits)
        scores = jnp.zeros((length, length), F32)
        for d, z_ref in enumerate((zf_ref, zb_ref)):
            mask = rows >= cols if d == 0 else rows <= cols
            z = z_ref[:, at].astype(F32)
            floor = floor_ref[d : d + 1, at]
            rest = 1.0 - floor
            logf = jnp.log(floor + rest * jax.nn.sigmoid(z)) + extra_ref[d, :, h : h + 1]
            key = rest * jax.nn.sigmoid(-z)
            running = dot(
                jnp.where(mask, 1.0, 0.0), logf, ((1,), (0,)), lax.Precision.HIGHEST
            )
            last = length - 1 if d == 0 else 0
            total = running[last : last + 1]
            centred = running - running[middle : middle + 1]
            part = dot(
                (queries * jnp.exp(centred)).astype(BF16),
                (key * jnp.exp(-centred)).astype(BF16),
                ((1,), (1,)),
            )
            scores += jnp.where(mask, part, 0.0)
            carry_ref[d, :, at] = (queries * jnp.exp(running)).astype(BF16)
            fresh = (key * jnp.exp(total - running)).astype(BF16)
            state_ref[d, h] = dot(values, fresh, ((0,), (0,))).astype(BF16)
            decay_ref[d, h] = jnp.broadcast_to(
                jnp.exp(total), (DECAY_ROWS, HEAD_WIDTH)
            ).astype(BF16)
        out_ref[:, at] = dot(scores.astype(BF16), values, ((1,), (0,)))


def prefix_kernel(rows, got_ref, out_ref):
    n = got_ref.shape[0]
    forward = lax.axis_index("sp") < n // 2

    def hop(k, carry):
        at = jnp.where(forward, k, n - 1 - k)
        out_ref[at] = carry.astype(BF16)
        block = got_ref[at].astype(F32)
        return block[rows : rows + 1] * carry + block[:rows]

    lax.fori_loop(0, n, hop, jnp.zeros((rows, HEAD_WIDTH), F32))


def finish_kernel(heads, out_ref, carry_ref, enter_ref, gate_ref, scale_ref, gated_ref):
    for h in range(heads):
        at = slice(h * HEAD_WIDTH, (h + 1) * HEAD_WIDTH)
        total = out_ref[:, at]
        for d in range(2):
            total += dot(carry_ref[d, :, at], enter_ref[d, h], ((1,), (1,)))
        mean = jnp.mean(total * total, axis=-1, keepdims=True)
        g = gate_ref[:, at].astype(F32)
        gated_ref[:, at] = (
            total * lax.rsqrt(mean + EPSILON) * scale_ref[...] * (g * jax.nn.sigmoid(g))
        ).astype(BF16)


def on_device(
    grid,
    residual,
    forget_forward,
    forget_backward,
    value_written,
    query_logits,
    output_gate_logits,
    forget_minimum,
    extra_log_rate,
    head_norm_scale,
    output_matrix,
    prenorm_scale,
    gate_up_matrix,
    value_up_matrix,
    gate_taps,
    value_taps,
    down_matrix,
):
    sp, tp = grid.sp, grid.x
    length, width = value_written.shape
    heads = width // HEAD_WIDTH
    depth, units = gate_up_matrix.shape
    unit = units // sp
    me = lax.axis_index("sp")

    out_full = lax.all_gather(output_matrix, "sp", axis=1, tiled=True)

    def cut(w):
        return w.reshape(depth, sp, unit).transpose(1, 0, 2)

    up = jnp.concatenate([cut(gate_up_matrix), cut(value_up_matrix)], axis=2)
    down = down_matrix.reshape(sp, unit, down_matrix.shape[1])
    up, down = exchange(grid, [(up, "sp"), (down, "sp")], True)
    up = up.reshape(sp * depth, 2 * unit)
    down = down.transpose(1, 0, 2).reshape(unit, -1)

    local, carry, state, decay = pl.pallas_call(
        functools.partial(local_kernel, heads),
        out_shape=(
            jax.ShapeDtypeStruct((length, width), F32),
            jax.ShapeDtypeStruct((2, length, width), BF16),
            jax.ShapeDtypeStruct((2, heads, HEAD_WIDTH, HEAD_WIDTH), BF16),
            jax.ShapeDtypeStruct((2, heads, DECAY_ROWS, HEAD_WIDTH), BF16),
        ),
    )(forget_forward, forget_backward, value_written, query_logits, forget_minimum, extra_log_rate)

    rows = 2 * heads * HEAD_WIDTH // sp
    decays = jnp.repeat(
        decay.reshape(2 * heads, DECAY_ROWS, HEAD_WIDTH), sp // (2 * heads), axis=0
    )
    message = jnp.concatenate([state.reshape(sp, rows, HEAD_WIDTH), decays], axis=1)
    (got,) = exchange(grid, [(message, "sp")], True)
    prefix = pl.pallas_call(
        functools.partial(prefix_kernel, rows),
        out_shape=jax.ShapeDtypeStruct((sp, rows, HEAD_WIDTH), BF16),
    )(got)
    (entering,) = exchange(grid, [(prefix, "sp")], True)
    gated = pl.pallas_call(
        functools.partial(finish_kernel, heads),
        out_shape=jax.ShapeDtypeStruct((length, width), BF16),
    )(
        local,
        carry,
        entering.reshape(2, heads, HEAD_WIDTH, HEAD_WIDTH),
        output_gate_logits,
        head_norm_scale[None],
    )
    (swapped,) = exchange(grid, [(gated.reshape(tp, length // tp, width), "x")], True)
    token_rows = swapped.transpose(1, 0, 2).reshape(length // tp, tp * width)
    mixed = jnp.dot(token_rows, out_full, preferred_element_type=F32)
    own_after = residual.astype(F32) + mixed
    mean = jnp.mean(own_after * own_after, axis=-1, keepdims=True)
    normed = (own_after * lax.rsqrt(mean + EPSILON) * prenorm_scale).astype(BF16)
    everyone = gather(grid, normed)
    tokens = everyone.reshape(-1, normed.shape[1])
    upward = jnp.dot(tokens, up, preferred_element_type=F32).astype(BF16)
    padded = jnp.pad(upward, ((1, 1), (0, 0)))
    taps = jnp.concatenate(
        [
            lax.dynamic_slice_in_dim(gate_taps, me * unit, unit, 1),
            lax.dynamic_slice_in_dim(value_taps, me * unit, unit, 1),
        ],
        axis=1,
    )
    count = tokens.shape[0]
    conv = padded[:count] * taps[0] + padded[1 : count + 1] * taps[1] + padded[2:] * taps[2]
    hidden = (jax.nn.silu(conv[:, :unit]) * conv[:, unit:]).astype(BF16)
    parts = hidden.reshape(everyone.shape[:-1] + (unit,))
    half = down.shape[1] // 2

    def project(order, weights):
        moved = parts.transpose(*order, 4, 5)
        product = jnp.dot(moved.reshape(-1, unit), weights, preferred_element_type=F32)
        return product.astype(BF16).reshape(moved.shape[:-1] + (weights.shape[1],))

    down_sum = reduce_scatter(
        grid, project((2, 3, 1, 0), down[:, :half]), project((2, 1, 3, 0), down[:, half:])
    )
    return (own_after + down_sum).astype(BF16)


def solution(mesh):
    return jax.shard_map(
        functools.partial(on_device, Grid(mesh)),
        mesh=mesh,
        in_specs=(
            P(("sp", "tp"), None),
            P("sp", "tp"),
            P("sp", "tp"),
            P("sp", "tp"),
            P("sp", "tp"),
            P("sp", "tp"),
            P(None, "tp"),
            P(None, "sp", "tp"),
            P(),
            P(None, "sp"),
            P(),
            P("sp", "tp"),
            P("sp", "tp"),
            P(None, "tp"),
            P(None, "tp"),
            P("tp", "sp"),
        ),
        out_specs=P(("sp", "tp"), None),
        check_vma=False,
    )
```

profile of v0, /device:TPU:0, one launch (start us, length us, event | category | flops | bytes accessed | tf_op | source)
XLA Modules:
  0.0 261.8 jit_solution(5455444308881877371)
XLA Ops:
  6.5 0.7 all-gather.2.cloned.1.call-update
  7.3 1.5 copy.18.extra_ref
  8.7 4.2 %shard_map.154 = (f32[128,512]{1,0:T(8,128)}, bf16[2,128,512]{2,1,0:T(8,128)(2,1)}, bf16[2,4,128,128]{3,2,1,0:T(8,128)(2,1)}, bf16[2,4,16,128]{3,2,1,0:T(8,128)(2,1)}) custom-call(bf16[128,512]{1,0:T(8,128)(2,1)} %zf_ref.1, bf16[128,512]{1,0:T(8,128)(2,1)} %zb_ref.1, bf16[128,512]{1,0:T(8,128)(2,1)} %v_ref.1, bf16[128,512]{1,0:T(8,128)(2,1)} %q_ref.1, ...), custom_call_target="tpu_custom_call" | custom-call | tf_op jit(solution)/shard_map/pallas_call | solution.py:421
  12.9 0.8 broadcast_in_dim.8
  13.7 1.7 pad_maximum_fusion.1.refs_0_
  15.4 13.9 %shard_map.155.got_ref = bf16[16,80,128]{2,1,0:T(8,128)(2,1)} custom-call(bf16[16,80,128]{2,1,0:T(8,128)(2,1)} %pad_maximum_fusion.1.refs_0_), custom_call_target="tpu_custom_call" | custom-call | tf_op jit(solution)/shard_map/pallas_call | solution.py:102
  29.3 1.9 shard_map.156.refs_0_
  31.2 18.0 %shard_map.157 = bf16[16,64,128]{2,1,0:T(8,128)(2,1)} custom-call(bf16[16,64,128]{2,1,0:T(8,128)(2,1)} %shard_map.156.refs_0_), custom_call_target="tpu_custom_call" | custom-call | tf_op jit(solution)/shard_map/pallas_call | solution.py:102
  49.2 2.3 shard_map.158
  51.5 4.6 %shard_map.159 = bf16[2,64,512]{2,1,0:T(8,128)(2,1)} custom-call(bf16[2,64,512]{2,1,0:T(8,128)(2,1)} %bitcast.51), custom_call_target="tpu_custom_call" | custom-call | tf_op jit(solution)/shard_map/pallas_call | solution.py:102
  56.1 1.6 copy.28
  57.6 0.3 copy.20
  58.0 0.5 copy.21
  58.5 0.3 copy.22
  58.9 0.5 copy.23
  59.4 1.8 pad_maximum_fusion.refs_0_
  61.2 52.2 %shard_map.161 = (bf16[16,128,352]{2,1,0:T(8,128)(2,1)}, bf16[16,176,128]{2,1,0:T(8,128)(2,1)}) custom-call(bf16[16,128,352]{2,1,0:T(8,128)(2,1)} %pad_maximum_fusion.refs_0_, bf16[16,176,128]{2,1,0:T(8,128)(2,1)} %bitcast.49), custom_call_target="tpu_custom_call" | custom-call | tf_op jit(solution)/shard_map/pallas_call | solution.py:102
  113.5 0.8 constant_dynamic-slice_fusion
  114.3 1.2 copy_bitcast_fusion
  115.6 3.2 %multiply_reduce_fusion = (f32[64]{0:T(128)S(1)}, f32[64,2048]{1,0:T(8,128)S(1)}) fusion(bf16[64,1024]{1,0:T(8,128)(2,1)S(1)} %bitcast.52, bf16[1024,2048]{1,0:T(8,128)(2,1)} %all-gather.2.cloned.1.call-done, bf16[64,2048]{1,0:T(8,128)(2,1)S(1)} %copy-done.3), kind=kOutput, calls=%fused_computation.11 | convolution fusion | flops 268959680 | bytes 5112064 | tf_op jit(solution)/shard_map/dot_general | solution.py:454
  118.8 0.8 multiply_convert_fusion.x_ref
  119.6 57.5 %shard_map.160 = bf16[4,2,2,2,64,2048]{5,4,3,2,1,0:T(8,128)(2,1)} custom-call(bf16[64,2048]{1,0:T(8,128)(2,1)} %multiply_convert_fusion.x_ref), custom_call_target="tpu_custom_call" | custom-call | tf_op jit(solution)/shard_map/pallas_call | solution.py:174
  177.1 6.6 %convolution_convert_fusion.2 = bf16[2048,352]{0,1:T(8,128)(2,1)S(1)} fusion(bf16[2048,2048]{1,0:T(8,128)(2,1)} %bitcast.41, bf16[2048,352]{1,0:T(8,128)(2,1)S(1)} %bitcast.57), kind=kOutput, calls=%fused_computation.3 | convolution fusion | flops 2953510912 | bytes 11272192 | tf_op jit(solution)/shard_map/dot_general | solution.py:460
  183.7 2.8 %multiply_add_fusion = f32[2048,352]{0,1:T(8,128)S(1)} fusion(bf16[2048,352]{0,1:T(8,128)(2,1)S(1)} %convolution_convert_fusion.2, f32[352]{0:T(512)S(1)} %get-tuple-element.19, f32[352]{0:T(512)S(1)} %get-tuple-element.18, f32[352]{0:T(512)S(1)} %get-tuple-element.17), kind=kLoop, calls=%fused_computation.2 | loop fusion | flops 5767168 | bytes 4329600 | tf_op jit(solution)/shard_map/add | solution.py:470
  186.6 0.4 fusion
  187.0 0.7 copy.24
  187.7 0.1 copy.27
  187.9 0.1 copy.25
  188.0 3.2 %convolution_convert_fusion.1 = bf16[2048,1024]{1,0:T(8,128)(2,1)} fusion(bf16[2048,176]{1,0:T(8,128)(2,1)S(1)} %bitcast.43, bf16[176,2048]{1,0:T(8,128)(2,1)S(1)} %copy_bitcast_fusion), kind=kOutput, calls=%fused_computation.1 | convolution fusion | flops 740294656 | bytes 5603328 | tf_op jit(solution)/shard_map/dot_general | solution.py:477
  191.1 3.2 %convolution_convert_fusion = bf16[2048,1024]{1,0:T(8,128)(2,1)} fusion(bf16[2048,176]{1,0:T(8,128)(2,1)S(1)} %bitcast.42, bf16[176,2048]{1,0:T(8,128)(2,1)S(1)} %copy_bitcast_fusion), kind=kOutput, calls=%fused_computation | convolution fusion | flops 740294656 | bytes 5603328 | tf_op jit(solution)/shard_map/dot_general | solution.py:477
  194.4 58.8 %shard_map.162 = f32[64,2048]{1,0:T(8,128)} custom-call(bf16[2,2,2,4,64,1024]{5,4,3,2,1,0:T(8,128)(2,1)} %bitcast.37, bf16[2,2,2,4,64,1024]{5,4,3,2,1,0:T(8,128)(2,1)} %bitcast.38), custom_call_target="tpu_custom_call" | custom-call | tf_op jit(solution)/shard_map/pallas_call | solution.py:294
  253.2 1.8 add_convert_fusion
  (16 shorter events, 0.2 us)
Async XLA Ops:
  6.5 51.1 %copy-start = (bf16[128,2816]{1,0:T(8,128)(2,1)S(1)}, bf16[128,2816]{1,0:T(8,128)(2,1)}, u32[]{:S(2)}) copy-start(bf16[128,2816]{1,0:T(8,128)(2,1)} %param.27) | copy-start | bytes 2162692
  6.5 109.0 %all-gather.2.cloned.1.call-start = ((), (), s32[]{:S(2)}) async-start(), calls=%async_computation | async-start | bytes 4456448 | tf_op jit(solution)/shard_map/all_gather | solution.py:410
  29.3 29.2 %copy-start.1 = (bf16[128,2816]{1,0:T(8,128)(2,1)S(1)}, bf16[128,2816]{1,0:T(8,128)(2,1)}, u32[]{:S(2)}) copy-start(bf16[128,2816]{1,0:T(8,128)(2,1)} %param.28) | copy-start | bytes 2162692
  59.4 56.2 %copy-start.2 = (bf16[2,8,8,512]{3,2,0,1:T(8,128)(2,1)S(1)}, bf16[2,8,8,512]{3,2,0,1:T(8,128)(2,1)}, u32[]{:S(2)}) copy-start(bf16[2,8,8,512]{3,2,0,1:T(8,128)(2,1)} %copy.28) | copy-start | bytes 393220
  59.4 56.2 %copy-start.3 = (bf16[64,2048]{1,0:T(8,128)(2,1)S(1)}, bf16[64,2048]{1,0:T(8,128)(2,1)}, u32[]{:S(2)}) copy-start(bf16[64,2048]{1,0:T(8,128)(2,1)} %param.16) | copy-start | bytes 786436
  115.5 3.2 %copy-start.4 = (f32[2048]{0:T(1024)S(1)}, f32[2048]{0:T(1024)}, u32[]{:S(2)}) copy-start(f32[2048]{0:T(1024)} %param.26) | copy-start | bytes 24580
  119.6 57.5 %copy-start.5 = (bf16[16,128,352]{2,1,0:T(8,128)(2,1)S(1)}, bf16[16,128,352]{2,1,0:T(8,128)(2,1)}, u32[]{:S(2)}) copy-start(bf16[16,128,352]{2,1,0:T(8,128)(2,1)} %get-tuple-element.15) | copy-start | bytes 4325380
Sparse Core Ops, SparseCore 0:
  9.5 62.3 all-gather.1
where the time goes:
time: 262 us
  Pallas kernels  213 us (81%)
  matrix products  16.2 us (6%)
  between operations  13.6 us (5%)
  other arithmetic  9.51 us (4%)
  local copies, waits for them, and re-layouts  8.45 us (3%)
    pallas_call x4, Pallas kernels, exchange(): pl.pallas_call(functools.partial(exchange_kernel, grid, dims, keep), out_...  88.7 us
    pallas_call x1, Pallas kernels, reduce_scatter(): pl.pallas_call(functools.partial(reduce_kernel, grid), out_shape=jax.Shap...  58.8 us
    pallas_call x1, Pallas kernels, gather(): pl.pallas_call(functools.partial(gather_kernel, grid), out_shape=jax.Shap...  57.5 us
    dot_general x1, matrix products, on_device(): upward = jnp.dot(tokens, up, preferred_element_type=F32).astype(BF16)  6.63 us
    dot_general x2, matrix products, project(): jnp.dot(moved.reshape(-1, unit), weights, preferred_element_type=F32)  6.4 us
  transfers between devices with their start and end apart: 1, of which 0 were waited for; matrix products, arithmetic and copies ran while one was open for 4% of the time, Pallas kernels for 37%

commit v1 on v0

--- a/solution.py
+++ b/solution.py
@@ -381,6 +381,669 @@
         ).astype(BF16)
 
 
+LANES = 128
+PAD_ROWS = 16
+SLICES = 4
+
+
+class Fused:
+    def __init__(self, grid, heads, length, depth, units, width):
+        self.grid = grid
+        self.heads, self.length, self.depth = heads, length, depth
+        self.quads = grid.z * grid.y
+        self.blocks = units // LANES
+        self.base = self.blocks // self.quads
+        self.most = -(-self.blocks // self.quads)
+        self.unit = self.most * LANES
+        self.width = width
+        self.rows = length // grid.x
+        self.shards = self.quads * grid.x
+        self.own = self.shards * self.rows
+        self.step = depth // (2 * SLICES)
+        self.quarter = width * grid.x // 4
+
+    @staticmethod
+    def fits(grid, heads, length, depth, units, width, out_depth):
+        return (
+            (grid.z, grid.y, grid.c, grid.x) == (4, 2, 2, 2)
+            and heads == grid.c * grid.y
+            and units % LANES == 0
+            and units // LANES >= grid.z * grid.y
+            and length % (16 * grid.x) == 0
+            and depth == out_depth == grid.sp * LANES
+            and depth % (2 * SLICES * LANES) == 0
+        )
+
+    def scratch(self):
+        g, h2, w = self.grid, HEAD_WIDTH + PAD_ROWS, HEAD_WIDTH
+        dma = pltpu.SemaphoreType.DMA
+        n = 2 * SLICES
+        tall = self.quads * g.x * self.rows
+        return dict(
+            wup=pltpu.VMEM((self.depth, 2 * self.unit), BF16),
+            wdn=pltpu.VMEM((self.unit, self.depth), BF16),
+            outm=pltpu.VMEM((g.z, g.y, self.width * g.x, g.c * LANES), BF16),
+            local=pltpu.VMEM((self.length, self.width), F32),
+            carry=pltpu.VMEM((2, self.length, self.width), BF16),
+            stb=pltpu.VMEM((2, 2, 2, h2, w), BF16),
+            rc=pltpu.VMEM((2, 2, h2, w), BF16),
+            ct=pltpu.VMEM((2, 2, h2, w), BF16),
+            ry=pltpu.VMEM((2, h2, w), BF16),
+            pt=pltpu.VMEM((2, h2, w), BF16),
+            rz=pltpu.VMEM((g.z, h2, w), BF16),
+            ce=pltpu.VMEM((2, 2, w, w), BF16),
+            yb=pltpu.VMEM((2, w, w), BF16),
+            ent=pltpu.VMEM((2, 2, 2, w, w), BF16),
+            cb=pltpu.VMEM((2, 2, w, w), BF16),
+            gb=pltpu.VMEM((self.rows, self.width), BF16),
+            sw=pltpu.VMEM((g.x, self.rows, self.width), BF16),
+            after=pltpu.VMEM((self.rows, self.depth), F32),
+            tok=pltpu.VMEM((g.z, g.y, g.x, self.rows, self.depth), BF16),
+            acc=pltpu.VMEM((tall, 2 * self.unit), F32),
+            ed=pltpu.VMEM((2 * self.most, 2 * self.quads, LANES), F32),
+            er=pltpu.VMEM((2 * self.most, 2 * self.quads + 16, LANES), F32),
+            hid=pltpu.VMEM((tall, self.unit), BF16),
+            part=pltpu.VMEM((g.z, g.y, g.x, self.rows, self.depth), BF16),
+            r1=pltpu.VMEM((n, g.z, 2, self.rows, self.step), BF16),
+            r2=pltpu.VMEM((n, g.z, self.rows, self.step), BF16),
+            r3=pltpu.VMEM((n, g.z - 1, self.rows, self.step), BF16),
+            loc_s=dma((2,)),
+            oz_s=dma((3, 4)), oz_r=dma((3, 4)),
+            oy_s=dma((3,)), oy_r=dma((3,)),
+            ox_s=dma((1,)), ox_r=dma((1,)),
+            oc_s=dma((4,)), oc_r=dma((4,)),
+            w_s=dma((self.quads, 6)), w_r=dma((self.quads, 6)),
+            f_s=dma((self.quads, 2)), f_r=dma((self.quads, 2)),
+            st_s=dma((5,)), st_r=dma((5,)),
+            sz_s=dma((3,)), sz_r=dma((3,)),
+            az_s=dma((n, 4)), az_r=dma((n, 4)),
+            a2_s=dma((n,)), a2_r=dma((n,)),
+            a3_s=dma((n,)), a3_r=dma((n,)),
+            ed_s=dma((1,)), ed_r=dma((1,)),
+            r1_s=dma((n,)), r1_r=dma((n,)),
+            r2_s=dma((n,)), r2_r=dma((n,)),
+            r3_s=dma((n, 3)), r3_r=dma((n, 3)),
+        )
+
+
+INPUTS = (
+    "zf",
+    "zb",
+    "val",
+    "qry",
+    "og",
+    "floor",
+    "extra",
+    "hscale",
+    "res",
+    "pscale",
+    "gtaps",
+    "vtaps",
+    "out_w",
+    "gate_w",
+    "value_w",
+    "down_w",
+)
+
+
+def fused_kernel(f, names, *refs):
+    R = dict(zip(INPUTS + ("out",) + tuple(names), refs))
+    R = type("Refs", (), R)
+    g = f.grid
+    s, x = lax.axis_index("sp"), lax.axis_index("tp")
+    c, y, z = lax.rem(s, 2), lax.rem(s // 2, 2), s // 4
+    q = s // 2
+    W, U, Q = HEAD_WIDTH, f.unit, f.quads
+    H, D = f.rows, f.depth
+    drains = []
+
+    def to(z=z, y=y, c=c, x=x):
+        return {"sp": (z * 2 + y) * 2 + c, "tp": x}
+
+    def remote(src, dst, ss, rs, dev):
+        return pltpu.make_async_remote_copy(
+            src_ref=src, dst_ref=dst, send_sem=ss, recv_sem=rs, device_id=dev, device_id_type=MESH
+        )
+
+    def go(cp, cond=None):
+        if cond is None:
+            cp.start()
+        else:
+            pl.when(cond)(cp.start)
+        drains.append((cond, cp))
+        return cp
+
+    def lane(i):
+        return pl.ds(pl.multiple_of(i * LANES, LANES), LANES)
+
+    def first_block(j):
+        return (f.blocks * j) // Q
+
+    def extra_block(j):
+        return first_block(j + 1) - first_block(j) > f.base
+
+    mine = first_block(q)
+    has_extra = extra_block(q)
+    main, rest = f.base * LANES, (f.most - f.base) * LANES
+
+    def weight_copies(src_s, j, kinds):
+        start = first_block(j)
+        at = pl.ds(pl.multiple_of(start * LANES, LANES), main)
+        at2 = pl.ds(pl.multiple_of((start + f.base) * LANES, LANES), LANES)
+        k = pl.ds(pl.multiple_of(src_s * LANES, LANES), LANES)
+        out = []
+        if "up" in kinds:
+            out.append((0, None, R.gate_w.at[:, at], R.wup.at[k, pl.ds(0, main)]))
+            out.append((1, None, R.value_w.at[:, at], R.wup.at[k, pl.ds(U, main)]))
+            if rest:
+                e = extra_block(j)
+                out.append((2, e, R.gate_w.at[:, at2], R.wup.at[k, pl.ds(main, LANES)]))
+                out.append((3, e, R.value_w.at[:, at2], R.wup.at[k, pl.ds(U + main, LANES)]))
+        if "down" in kinds:
+            out.append((4, None, R.down_w.at[at, :], R.wdn.at[pl.ds(0, main), k]))
+            if rest:
+                out.append((5, extra_block(j), R.down_w.at[at2, :], R.wdn.at[pl.ds(main, LANES), k]))
+        return out
+
+    def own_weights(kinds):
+        for i, cond, src, dst in weight_copies(s, q, kinds):
+            cp = pltpu.make_async_copy(src, dst, R.w_r.at[q, i])
+            if cond is None:
+                cp.start()
+            else:
+                pl.when(cond)(cp.start)
+
+    def send_weights(k, kinds):
+        j = lax.rem(q + k, Q)
+        for i, cond, src, dst in weight_copies(s, j, kinds):
+            go(remote(src, dst, R.w_s.at[k, i], R.w_r.at[q, i], {"sp": j * 2 + c, "tp": x}), cond)
+
+    def pass_weights(p, kinds):
+        ps = p * 2 + c
+        for i, cond, _, dst in weight_copies(ps, q, kinds):
+            cp = remote(dst, dst, R.w_s.at[0, i], R.w_r.at[p, i], to(c=1 - c))
+            if cond is None:
+                cp.wait_recv()
+            else:
+                pl.when(cond)(cp.wait_recv)
+        k = pl.ds(pl.multiple_of(ps * LANES, LANES), LANES)
+        if "up" in kinds:
+            go(remote(R.wup.at[k, :], R.wup.at[k, :], R.f_s.at[p, 0], R.f_r.at[p, 0], to(c=1 - c)))
+        if "down" in kinds:
+            go(remote(R.wdn.at[:, k], R.wdn.at[:, k], R.f_s.at[p, 1], R.f_r.at[p, 1], to(c=1 - c)))
+
+    def wait_weights(p, kind):
+        k = pl.ds(pl.multiple_of((p * 2 + 1 - c) * LANES, LANES), LANES)
+        ref = R.wup.at[k, :] if kind == 0 else R.wdn.at[:, k]
+        remote(ref, ref, R.f_s.at[p, kind], R.f_r.at[p, kind], to(c=1 - c)).wait_recv()
+
+    mid = (z == 1) | (z == 2)
+    t0, t1 = jnp.where(z == 1, 0, 1), jnp.where(z == 2, 3, 2)
+    far = jnp.where(z == 1, 0, 3)
+
+    class ZGather:
+        def __init__(self, src, dst, ss, rs):
+            self.src, self.dst, self.ss, self.rs = src, dst, ss, rs
+
+        def start(self):
+            for j, t in enumerate((t0, t1)):
+                go(remote(self.src, self.dst(z), self.ss(j), self.rs(z), to(z=t)))
+
+        def arrive(self, shard):
+            d = self.dst(shard)
+            remote(d, d, self.ss(0), self.rs(shard), to(z=t0)).wait_recv()
+
+        def forward(self):
+            for k in range(2):
+                shard = jnp.where(z == 1, 2 + k, k)
+                d = self.dst(shard)
+                cp = remote(d, d, self.ss(2 + k), self.rs(shard), to(z=far))
+
+                @pl.when(mid)
+                def _(cp=cp):
+                    cp.wait_recv()
+                    cp.start()
+
+                drains.append((mid, cp))
+
+        def finish(self):
+            @pl.when(mid)
+            def _():
+                self.arrive(far)
+
+            @pl.when(jnp.logical_not(mid))
+            def _():
+                for k in range(3):
+                    self.arrive(jnp.where(z == 0, 1 + k, k))
+
+    if rest:
+        @pl.when(jnp.logical_not(has_extra))
+        def _():
+            R.wup[:, main:U] = jnp.zeros((D, LANES), BF16)
+            R.wup[:, U + main :] = jnp.zeros((D, LANES), BF16)
+            R.wdn[main:U, :] = jnp.zeros((LANES, D), BF16)
+
+    edge = jnp.zeros((2 * f.most, 8, LANES), F32)
+    R.er[:, 0:8, :] = edge
+    R.er[:, 8 + 2 * Q :, :] = edge
+
+    barrier = pltpu.get_barrier_semaphore()
+    for k in range(1, Q):
+        dev = {"sp": lax.rem(q + k, Q) * 2 + c, "tp": x}
+        pl.semaphore_signal(barrier, inc=1, device_id=dev, device_id_type=MESH)
+    pl.semaphore_signal(barrier, inc=1, device_id=to(c=1 - c), device_id_type=MESH)
+    pl.semaphore_signal(barrier, inc=1, device_id=to(x=1 - x), device_id_type=MESH)
+    pl.semaphore_wait(barrier, Q + 1)
+
+    ccol = lane(c)
+    O = f.quarter
+    starts = (2 * O + x * O, 0, O)
+    own_out = []
+    for i, (r, size) in enumerate(((starts[0], O), (0, 2 * O))):
+        at = pl.ds(pl.multiple_of(r, O), size)
+        cp = pltpu.make_async_copy(R.out_w.at[at, :], R.outm.at[z, y, at, ccol], R.loc_s.at[i])
+        cp.start()
+        own_out.append(cp)
+    zg = []
+    for i, r in enumerate(starts):
+        at = pl.ds(pl.multiple_of(r, O), O)
+        zg.append(
+            ZGather(
+                R.out_w.at[at, :],
+                lambda k, at=at: R.outm.at[k, y, at, ccol],
+                lambda j, i=i: R.oz_s.at[i, j],
+                lambda j, i=i: R.oz_r.at[i, j],
+            )
+        )
+        zg[-1].start()
+
+    def out_y(i):
+        at = pl.ds(pl.multiple_of(starts[i], O), O)
+        src = R.outm.at[:, y, at, ccol]
+        return remote(src, src, R.oy_s.at[i], R.oy_r.at[i], to(y=1 - y))
+
+    def out_x():
+        at = pl.ds(pl.multiple_of(starts[0], O), O)
+        src = R.outm.at[:, :, at, ccol]
+        return remote(src, src, R.ox_s.at[0], R.ox_r.at[0], to(x=1 - x))
+
+    def out_c(i):
+        src = R.outm.at[:, :, pl.ds(i * O, O), ccol]
+        return remote(src, src, R.oc_s.at[i], R.oc_r.at[i], to(c=1 - c))
+
+    own_weights(("up",))
+    send_weights(1, ("up",))
+
+    L = f.length
+    rows_i = lax.broadcasted_iota(jnp.int32, (L, L), 0)
+    cols_i = lax.broadcasted_iota(jnp.int32, (L, L), 1)
+    middle = L // 2
+    for h in range(f.heads):
+        at = slice(h * W, (h + 1) * W)
+        values = R.val[:, at]
+        logits = R.qry[:, at].astype(F32)
+        queries = logits * jax.nn.sigmoid(logits)
+        scores = jnp.zeros((L, L), F32)
+        for d, z_ref in enumerate((R.zf, R.zb)):
+            mask = rows_i >= cols_i if d == 0 else rows_i <= cols_i
+            pre = z_ref[:, at].astype(F32)
+            floor = R.floor[d : d + 1, at]
+            span = 1.0 - floor
+            logf = jnp.log(floor + span * jax.nn.sigmoid(pre)) + R.extra[d, :, h : h + 1]
+            key = span * jax.nn.sigmoid(-pre)
+            running = dot(jnp.where(mask, 1.0, 0.0), logf, ((1,), (0,)), lax.Precision.HIGHEST)
+            last = L - 1 if d == 0 else 0
+            total = running[last : last + 1]
+            centred = running - running[middle : middle + 1]
+            inner = dot(
+                (queries * jnp.exp(centred)).astype(BF16),
+                (key * jnp.exp(-centred)).astype(BF16),
+                ((1,), (1,)),
+            )
+            scores += jnp.where(mask, inner, 0.0)
+            R.carry[d, :, at] = (queries * jnp.exp(running)).astype(BF16)
+            fresh = (key * jnp.exp(total - running)).astype(BF16)
+            R.stb[h // 2, h % 2, d, :W] = dot(values, fresh, ((0,), (0,))).astype(BF16)
+            R.stb[h // 2, h % 2, d, W:] = jnp.broadcast_to(jnp.exp(total), (PAD_ROWS, W)).astype(BF16)
+        R.local[:, at] = dot(scores.astype(BF16), values, ((1,), (0,)))
+
+    def state(ref, *at):
+        return ref[at + (slice(0, W),)].astype(F32)
+
+    def decay(ref, *at):
+        return ref[at + (slice(W, W + 1),)].astype(F32)
+
+    def put(ref, at, value, factor):
+        ref[at + (slice(0, W),)] = value.astype(BF16)
+        ref[at + (slice(W, W + PAD_ROWS),)] = jnp.broadcast_to(factor, (PAD_ROWS, W)).astype(BF16)
+
+    def hop(i, src, dst, dev):
+        return go(remote(src, dst, R.st_s.at[i], R.st_r.at[i], dev))
+
+    step = hop(0, R.stb.at[1 - c], R.rc, to(c=1 - c))
+    for o in zg:
+        o.forward()
+    send_weights(2, ("up",))
+    step.wait_recv()
+    for hp in range(2):
+        for d in range(2):
+            ahead = c == d
+            so, ao = state(R.stb, c, hp, d), decay(R.stb, c, hp, d)
+            sp_, ap = state(R.rc, hp, d), decay(R.rc, hp, d)
+            both = jnp.where(ahead, ap, ao) * jnp.where(ahead, so, sp_) + jnp.where(ahead, sp_, so)
+            put(R.ct, (hp, d), both, ao * ap)
+    step = hop(1, R.ct.at[1 - y], R.ry, to(y=1 - y))
+    for cp in own_out:
+        cp.wait()
+    out_ys = []
+    for i, o in enumerate(zg):
+        o.finish()
+        out_ys.append(go(out_y(i)))
+    send_weights(7, ("up",))
+    step.wait_recv()
+    for d in range(2):
+        ahead = y == d
+        so, ao = state(R.ct, y, d), decay(R.ct, y, d)
+        sp_, ap = state(R.ry, d), decay(R.ry, d)
+        both = jnp.where(ahead, ap, ao) * jnp.where(ahead, so, sp_) + jnp.where(ahead, sp_, so)
+        put(R.pt, (d,), both, ao * ap)
+    hops = []
+    for k in range(1, 4):
+        zt = lax.rem(z + k, 4)
+        src = R.pt.at[jnp.where(zt > z, 0, 1)]
+        hops.append(go(remote(src, R.rz.at[z], R.sz_s.at[k - 1], R.sz_r.at[k - 1], to(z=zt))))
+    out_ys[0].wait_recv()
+    out_xs = go(out_x())
+    send_weights(6, ("up",))
+    send_weights(3, ("up",))
+    for h_ in hops:
+        h_.wait_recv()
+
+    def enter(d):
+        def one(i, e):
+            at = i if d == 0 else 3 - i
+            return decay(R.rz, at) * e + state(R.rz, at)
+
+        return lax.fori_loop(0, z if d == 0 else 3 - z, one, jnp.zeros((W, W), F32))
+
+    for d in range(2):
+        e = enter(d)
+        so, ao = state(R.ct, y, d), decay(R.ct, y, d)
+        sp_, ap = state(R.ry, d), decay(R.ry, d)
+        R.ce[y, d] = jnp.where(y == d, e, ap * e + sp_).astype(BF16)
+        R.yb[d] = jnp.where(y == d, ao * e + so, e).astype(BF16)
+    step = hop(2, R.yb, R.ce.at[y], to(y=1 - y))
+    out_cs = []
+    for i in (1, 2):
+        out_ys[i].wait_recv()
+        out_cs.append(go(out_c(i - 1)))
+    send_weights(5, ("up",))
+    send_weights(4, ("up",))
+    step.wait_recv()
+    for hp in range(2):
+        for d in range(2):
+            e = R.ce[hp, d].astype(F32)
+            so, ao = state(R.stb, c, hp, d), decay(R.stb, c, hp, d)
+            sp_, ap = state(R.rc, hp, d), decay(R.rc, hp, d)
+            R.ent[c, hp, d] = jnp.where(c == d, e, ap * e + sp_).astype(BF16)
+            R.cb[hp, d] = jnp.where(c == d, ao * e + so, e).astype(BF16)
+    step = hop(3, R.cb, R.ent.at[c], to(c=1 - c))
+    out_xs.wait_recv()
+    for i in (2, 3):
+        out_cs.append(go(out_c(i)))
+    step.wait_recv()
+
+    def finish(half, write):
+        at_rows = pl.ds(pl.multiple_of(half * H, H), H)
+        for h in range(f.heads):
+            at = slice(h * W, (h + 1) * W)
+            total = R.local[at_rows, at]
+            for d in range(2):
+                total += dot(R.carry[d, at_rows, at], R.ent[h // 2, h % 2, d], ((1,), (1,)))
+            mean = jnp.mean(total * total, axis=-1, keepdims=True)
+            gate = R.og[at_rows, at].astype(F32)
+            write(
+                at,
+                (
+                    total * lax.rsqrt(mean + EPSILON) * R.hscale[...] * (gate * jax.nn.sigmoid(gate))
+                ).astype(BF16),
+            )
+
+    def write_peer(at, value):
+        R.gb[:, at] = value
+
+    def write_own(at, value):
+        R.sw[x, :, at] = value
+
+    finish(1 - x, write_peer)
+    step = hop(4, R.gb, R.sw.at[x], to(x=1 - x))
+    finish(x, write_own)
+    for o in out_cs:
+        o.wait_recv()
+    step.wait_recv()
+    square = jnp.zeros((H, 1), F32)
+    width = g.c * LANES
+    for p in range(Q):
+        at = slice(p * width, (p + 1) * width)
+        total = R.res[:, at].astype(F32)
+        for t in range(2):
+            total += dot(R.sw[t], R.outm[p // 2, p % 2, t * f.width : (t + 1) * f.width], ((1,), (0,)))
+        R.after[:, at] = total
+        square += jnp.sum(total * total, axis=-1, keepdims=True)
+    scale = lax.rsqrt(square / D + EPSILON)
+    for p in range(Q):
+        at = slice(p * width, (p + 1) * width)
+        R.tok[z, y, x, :, at] = (R.after[:, at] * scale * R.pscale[:, at]).astype(BF16)
+
+    n, S = 2 * SLICES, f.step
+
+    def cols(k):
+        return slice(k * S, (k + 1) * S)
+
+    def cds(k):
+        return pl.ds(k * S, S)
+
+    ag = []
+    for k in range(n):
+        ag.append(
+            ZGather(
+                R.tok.at[z, y, x, :, cds(k)],
+                lambda t, k=k: R.tok.at[t, y, x, :, cds(k)],
+                lambda j, k=k: R.az_s.at[k, j],
+                lambda j, k=k: R.az_r.at[k, j],
+            )
+        )
+
+    def pair(t):
+        return (t, t + SLICES)
+
+    def second(k):
+        src = R.tok.at[:, y, x, :, cds(k)]
+        dev = to(x=1 - x) if k < SLICES else to(y=1 - y)
+        return remote(src, src, R.a2_s.at[k], R.a2_r.at[k], dev)
+
+    def third(k):
+        if k < SLICES:
+            src, dev = R.tok.at[:, y, :, :, cds(k)], to(y=1 - y)
+        else:
+            src, dev = R.tok.at[:, :, x, :, cds(k)], to(x=1 - x)
+        return remote(src, src, R.a3_s.at[k], R.a3_r.at[k], dev)
+
+    def up(k, first):
+        wait_weights(k, 0)
+        tall = g.y * g.x * H
+
+        def body(i, _):
+            at = pl.ds(pl.multiple_of(i * tall, tall), tall)
+            value = dot(R.tok[i, :, :, :, cols(k)].reshape(tall, S), R.wup[cols(k), :], ((1,), (0,)))
+            R.acc[at, :] = value if first else R.acc[at, :] + value
+            return 0
+
+        lax.fori_loop(0, g.z, body, 0)
+
+    for t in range(SLICES):
+        for k in pair(t):
+            ag[k].start()
+    own_weights(("down",))
+    flying = {}
+    for t in range(SLICES + 3):
+        if t < SLICES:
+            for k in pair(t):
+                ag[k].forward()
+        if 0 <= t - 1 < SLICES:
+            for k in pair(t - 1):
+                ag[k].finish()
+                flying[2, k] = go(second(k))
+        if t < SLICES:
+            pass_weights(2 * t, ("up",))
+            pass_weights(2 * t + 1, ("up",))
+            send_weights(2 * t + 1, ("down",))
+            if 2 * t + 2 < Q:
+                send_weights(2 * t + 2, ("down",))
+        if 0 <= t - 2 < SLICES:
+            for k in pair(t - 2):
+                flying[2, k].wait_recv()
+                flying[3, k] = go(third(k))
+        if 0 <= t - 3 < SLICES:
+            for k in pair(t - 3):
+                flying[3, k].wait_recv()
+                up(k, k == 0)
+
+    for i in range(Q):
+        for e, row in enumerate((i * L, (i + 1) * L - 1)):
+            value = R.acc[row : row + 1, :].astype(BF16).astype(F32)
+            for b in range(2 * f.most):
+                R.ed[b, 2 * i + e : 2 * i + e + 1, :] = value[:, b * LANES : (b + 1) * LANES]
+    edges = go(
+        remote(R.ed, R.er.at[:, pl.ds(8, 2 * Q), :], R.ed_s.at[0], R.ed_r.at[0], to(c=1 - c))
+    )
+    for p in range(Q):
+        pass_weights(p, ("down",))
+    edges.wait_recv()
+    top = lax.broadcasted_iota(jnp.int32, (L, LANES), 0)
+
+    def conv(i, _):
+        at = pl.ds(pl.multiple_of(i * L, L), L)
+        for b in range(f.most):
+            def branch(ref, off):
+                col = slice(off + b * LANES, off + (b + 1) * LANES)
+                tap = ref[:, pl.ds(pl.multiple_of((mine + b) * LANES, LANES), LANES)]
+                value = R.acc[at, col].astype(BF16).astype(F32)
+                before = R.er[off // LANES + b, pl.ds(7 + 2 * (i + c), 1), :]
+                behind = R.er[off // LANES + b, pl.ds(8 + 2 * (i + c), 1), :]
+                above = jnp.where(top == 0, before, pltpu.roll(value, 1, 0))
+                below = jnp.where(top == L - 1, behind, pltpu.roll(value, L - 1, 0))
+                return above * tap[0:1] + value * tap[1:2] + below * tap[2:3]
+
+            gate = branch(R.gtaps, 0)
+            value = branch(R.vtaps, U)
+            R.hid[at, b * LANES : (b + 1) * LANES] = (
+                gate * jax.nn.sigmoid(gate) * value
+            ).astype(BF16)
+        return 0
+
+    lax.fori_loop(0, Q, conv, 0)
+    for p in range(Q):
+        wait_weights(p, 1)
+
+    def down(k):
+        tall = g.y * g.x * H
+
+        def body(i, _):
+            at = pl.ds(pl.multiple_of(i * tall, tall), tall)
+            value = dot(R.hid[at, :], R.wdn[:, cols(k)], ((1,), (0,)))
+            R.part[i, :, :, :, cols(k)] = value.astype(BF16).reshape(g.y, g.x, H, S)
+            return 0
+
+        lax.fori_loop(0, g.z, body, 0)
+
+    def first_sum(k):
+        if k < SLICES:
+            src, dev = R.part.at[:, 1 - y, :, :, cds(k)], to(y=1 - y)
+        else:
+            src, dev = R.part.at[:, :, 1 - x, :, cds(k)], to(x=1 - x)
+        return remote(src, R.r1.at[k], R.r1_s.at[k], R.r1_r.at[k], dev)
+
+    def second_sum(k):
+        if k < SLICES:
+            src, dev = R.part.at[:, y, 1 - x, :, cds(k)], to(x=1 - x)
+        else:
+            src, dev = R.part.at[:, 1 - y, x, :, cds(k)], to(y=1 - y)
+        return remote(src, R.r2.at[k], R.r2_s.at[k], R.r2_r.at[k], dev)
+
+    def add_first(k):
+        def body(i, _):
+            zi, j = i // 2, lax.rem(i, 2)
+            at = (zi, y, j) if k < SLICES else (zi, j, x)
+            at = at + (slice(None), cols(k))
+            R.part[at] = (R.part[at].astype(F32) + R.r1[k, zi, j].astype(F32)).astype(BF16)
+            return 0
+
+        lax.fori_loop(0, 2 * g.z, body, 0)
+
+    def add_second(k):
+        def body(i, _):
+            at = (i, y, x, slice(None), cols(k))
+            R.part[at] = (R.part[at].astype(F32) + R.r2[k, i].astype(F32)).astype(BF16)
+            return 0
+
+        lax.fori_loop(0, g.z, body, 0)
+
+    def last_sums(k):
+        sums = []
+        for j in range(1, 4):
+            zt = lax.rem(z + j, 4)
+            src = R.part.at[zt, y, x, :, cds(k)]
+            sums.append(
+                go(remote(src, R.r3.at[k, j - 1], R.r3_s.at[k, j - 1], R.r3_r.at[k, j - 1], to(z=zt)))
+            )
+        return sums
+
+    for t in range(SLICES):
+        for k in pair(t):
+            down(k)
+            flying[4, k] = go(first_sum(k))
+    for t in range(1, SLICES + 3):
+        if t - 1 < SLICES:
+            for k in pair(t - 1):
+                flying[4, k].wait_recv()
+                add_first(k)
+                flying[5, k] = go(second_sum(k))
+        if 0 <= t - 2 < SLICES:
+            for k in pair(t - 2):
+                flying[5, k].wait_recv()
+                add_second(k)
+                flying[6, k] = last_sums(k)
+        if 0 <= t - 3 < SLICES:
+            for k in pair(t - 3):
+                total = R.after[:, cols(k)] + R.part[z, y, x, :, cols(k)].astype(F32)
+                for j, cp in enumerate(flying[6, k]):
+                    cp.wait_recv()
+                    total += R.r3[k, j].astype(F32)
+                R.out[:, cols(k)] = total.astype(BF16)
+    for cond, cp in drains:
+        if cond is None:
+            cp.wait_send()
+        else:
+            pl.when(cond)(cp.wait_send)
+
+
+def fused(grid, f, args):
+    scratch = f.scratch()
+    vmem = pl.BlockSpec(memory_space=pltpu.VMEM)
+    anyw = pl.BlockSpec(memory_space=pl.ANY)
+    return pl.pallas_call(
+        functools.partial(fused_kernel, f, list(scratch)),
+        out_shape=jax.ShapeDtypeStruct((f.rows, f.depth), BF16),
+        in_specs=[vmem] * 12 + [anyw] * 4,
+        out_specs=vmem,
+        scratch_shapes=list(scratch.values()),
+        compiler_params=pltpu.CompilerParams(
+            collective_id=next(grid.ids), has_side_effects=True, vmem_limit_bytes=60000000
+        ),
+    )(*args)
+
+
 def on_device(
     grid,
     residual,
@@ -400,6 +1063,36 @@
     value_taps,
     down_matrix,
 ):
+    shape = (
+        value_written.shape[1] // HEAD_WIDTH,
+        value_written.shape[0],
+        gate_up_matrix.shape[0] * grid.sp,
+        gate_up_matrix.shape[1],
+        value_written.shape[1],
+    )
+    if Fused.fits(grid, *shape, output_matrix.shape[1] * grid.sp):
+        return fused(
+            grid,
+            Fused(grid, *shape),
+            (
+                forget_forward,
+                forget_backward,
+                value_written,
+                query_logits,
+                output_gate_logits,
+                forget_minimum,
+                extra_log_rate,
+                head_norm_scale[None],
+                residual,
+                prenorm_scale[None],
+                gate_taps,
+                value_taps,
+                output_matrix,
+                gate_up_matrix,
+                value_up_matrix,
+                down_matrix,
+            ),
+        )
     sp, tp = grid.sp, grid.x
     length, width = value_written.shape
     heads = width // HEAD_WIDTH

time: 262 us -> 176 us (0.67)
  Pallas kernels: 213 us -> 173 us
  matrix products: 16.2 us -> 0 us
  between operations: 13.6 us -> 0.01 us
  other arithmetic: 9.51 us -> 0 us
  local copies, waits for them, and re-layouts: 8.45 us -> 3.15 us
    pallas_call x9 -> x1, Pallas kernels: 213 us -> 173 us  [fused(): pl.pallas_call(functools.partial(fused_kernel, f, list(scratch)), out_sha...]
    dot_general x4 -> x0, matrix products: 16.2 us -> none  [the longest x1 6.63 us: on_device(): upward = jnp.dot(tokens, up, preferred_element_type=F32).astype(BF16)]
    reshape x4 -> x0, local copies, waits for them, and re-layouts: 3.76 us -> none  [the longest x1 1.57 us: on_device(): token_rows = swapped.transpose(1, 0, 2).reshape(length // tp, tp * width)]
    concatenate x2 -> x0, other arithmetic: 3.52 us -> none  [the longest x1 1.81 us: on_device(): up = jnp.concatenate([cut(gate_up_matrix), cut(value_up_matrix)], axis=2)]
    convert_element_type x3 -> x0, other arithmetic: 3.06 us -> none  [the longest x1 1.82 us: on_device(): return (own_after + down_sum).astype(BF16)]
    add x1 -> x0, other arithmetic: 2.83 us -> none  [on_device(): padded[:count] * taps[0] + padded[1:count + 1] * taps[1]]
  transfers between devices with their start and end apart: 1 -> 0, of which waited for: 0 -> 0; matrix products, arithmetic and copies ran while one was open for 4% -> 0% of each run, Pallas kernels for 37% -> 0%
where the time goes in v1:
time: 176 us
  Pallas kernels  173 us (98%)
  local copies, waits for them, and re-layouts  3.15 us (2%)
    pallas_call x1, Pallas kernels, fused(): pl.pallas_call(functools.partial(fused_kernel, f, list(scratch)), out_sha...  173 us

profile of v1, /device:TPU:0, one launch (start us, length us, event | category | flops | bytes accessed | tf_op | source)
XLA Modules:
  0.0 176.2 jit_solution(16278080992008436314)
XLA Ops:
  0.0 1.5 copy.17.refs_6_
  1.5 173.1 %shard_map.154 = bf16[64,2048]{1,0:T(8,128)(2,1)} custom-call(bf16[128,512]{1,0:T(8,128)(2,1)} %refs_0_.1, bf16[128,512]{1,0:T(8,128)(2,1)} %refs_1_.1, bf16[128,512]{1,0:T(8,128)(2,1)} %refs_2_.1, bf16[128,512]{1,0:T(8,128)(2,1)} %refs_3_.1, bf16[128,512]{1,0:T(8,128)(2,1)} %refs_4_.1, f32[2,512]{1,0:T(2,128)} %refs_5_.1, f32[2,128,4]{2,1,0:T(8,128)} %copy.17.refs_6_, ...), custom_call_target="tpu_custom_call" | custom-call | tf_op jit(solution)/shard_map/pallas_call | solution.py:1035
  174.5 1.7 copy.19

commit v2 on v1

--- a/solution.py
+++ b/solution.py
@@ -383,7 +383,9 @@
 
 LANES = 128
 PAD_ROWS = 16
-SLICES = 4
+GATHER_WIDTHS = (2, 2, 2, 2)
+REDUCE_WIDTHS = (3, 2, 2, 1)
+OUT_PIECES = 4
 
 
 class Fused:
@@ -399,8 +401,19 @@
         self.rows = length // grid.x
         self.shards = self.quads * grid.x
         self.own = self.shards * self.rows
-        self.step = depth // (2 * SLICES)
-        self.quarter = width * grid.x // 4
+        self.gather = self.split(GATHER_WIDTHS)
+        self.reduce = self.split(REDUCE_WIDTHS)
+        self.piece = width // OUT_PIECES
+
+    def split(self, widths):
+        unit = self.depth // 2 // sum(widths)
+        out = []
+        for color in range(2):
+            first = color * (self.depth // 2)
+            for w in widths:
+                out.append((first, w * unit))
+                first += w * unit
+        return out
 
     @staticmethod
     def fits(grid, heads, length, depth, units, width, out_depth):
@@ -411,18 +424,20 @@
             and units // LANES >= grid.z * grid.y
             and length % (16 * grid.x) == 0
             and depth == out_depth == grid.sp * LANES
-            and depth % (2 * SLICES * LANES) == 0
+            and depth % (2 * LANES * sum(GATHER_WIDTHS)) == 0
+            and depth % (2 * LANES * sum(REDUCE_WIDTHS)) == 0
+            and width % (16 * OUT_PIECES) == 0
         )
 
     def scratch(self):
         g, h2, w = self.grid, HEAD_WIDTH + PAD_ROWS, HEAD_WIDTH
         dma = pltpu.SemaphoreType.DMA
-        n = 2 * SLICES
+        n, m = len(self.gather), len(self.reduce)
         tall = self.quads * g.x * self.rows
         return dict(
             wup=pltpu.VMEM((self.depth, 2 * self.unit), BF16),
             wdn=pltpu.VMEM((self.unit, self.depth), BF16),
-            outm=pltpu.VMEM((g.z, g.y, self.width * g.x, g.c * LANES), BF16),
+            outm=pltpu.VMEM((g.z, g.y, self.width, g.c * LANES), BF16),
             local=pltpu.VMEM((self.length, self.width), F32),
             carry=pltpu.VMEM((2, self.length, self.width), BF16),
             stb=pltpu.VMEM((2, 2, 2, h2, w), BF16),
@@ -435,8 +450,9 @@
             yb=pltpu.VMEM((2, w, w), BF16),
             ent=pltpu.VMEM((2, 2, 2, w, w), BF16),
             cb=pltpu.VMEM((2, 2, w, w), BF16),
-            gb=pltpu.VMEM((self.rows, self.width), BF16),
-            sw=pltpu.VMEM((g.x, self.rows, self.width), BF16),
+            gb=pltpu.VMEM((self.length, self.width), BF16),
+            xb=pltpu.VMEM((self.rows, self.depth), BF16),
+            xr=pltpu.VMEM((self.rows, self.depth), BF16),
             after=pltpu.VMEM((self.rows, self.depth), F32),
             tok=pltpu.VMEM((g.z, g.y, g.x, self.rows, self.depth), BF16),
             acc=pltpu.VMEM((tall, 2 * self.unit), F32),
@@ -444,28 +460,34 @@
             er=pltpu.VMEM((2 * self.most, 2 * self.quads + 16, LANES), F32),
             hid=pltpu.VMEM((tall, self.unit), BF16),
             part=pltpu.VMEM((g.z, g.y, g.x, self.rows, self.depth), BF16),
-            r1=pltpu.VMEM((n, g.z, 2, self.rows, self.step), BF16),
-            r2=pltpu.VMEM((n, g.z, self.rows, self.step), BF16),
-            r3=pltpu.VMEM((n, g.z - 1, self.rows, self.step), BF16),
-            loc_s=dma((2,)),
-            oz_s=dma((3, 4)), oz_r=dma((3, 4)),
-            oy_s=dma((3,)), oy_r=dma((3,)),
-            ox_s=dma((1,)), ox_r=dma((1,)),
-            oc_s=dma((4,)), oc_r=dma((4,)),
+            r1=pltpu.VMEM((g.z, 2, self.rows, self.depth), BF16),
+            r2=pltpu.VMEM((g.z, self.rows, self.depth), BF16),
+            r3=pltpu.VMEM((g.z - 1, self.rows, self.depth), BF16),
+            loc_s=dma((1,)),
+            oz_s=dma((OUT_PIECES, 4)), oz_r=dma((OUT_PIECES, 4)),
+            oy_s=dma((OUT_PIECES,)), oy_r=dma((OUT_PIECES,)),
+            oc_s=dma((OUT_PIECES,)), oc_r=dma((OUT_PIECES,)),
+            xs_s=dma((4,)), xs_r=dma((4,)),
+            su=pltpu.VMEM((g.z - 1, LANES, 2 * self.unit), BF16),
+            sd=pltpu.VMEM((g.z - 1, self.unit, LANES), BF16),
+            sy_s=dma((g.z, 6)), sy_r=dma((g.z, 6)),
             w_s=dma((self.quads, 6)), w_r=dma((self.quads, 6)),
             f_s=dma((self.quads, 2)), f_r=dma((self.quads, 2)),
-            st_s=dma((5,)), st_r=dma((5,)),
+            st_s=dma((4,)), st_r=dma((4,)),
             sz_s=dma((3,)), sz_r=dma((3,)),
             az_s=dma((n, 4)), az_r=dma((n, 4)),
             a2_s=dma((n,)), a2_r=dma((n,)),
             a3_s=dma((n,)), a3_r=dma((n,)),
             ed_s=dma((1,)), ed_r=dma((1,)),
-            r1_s=dma((n,)), r1_r=dma((n,)),
-            r2_s=dma((n,)), r2_r=dma((n,)),
-            r3_s=dma((n, 3)), r3_r=dma((n, 3)),
+            r1_s=dma((m,)), r1_r=dma((m,)),
+            r2_s=dma((m,)), r2_r=dma((m,)),
+            r3_s=dma((m, 3)), r3_r=dma((m, 3)),
         )
 
 
+NEAR = [(0, 0), (0, 1)]
+STRAIGHT = [(1, 0), (3, 0), (2, 0)]
+CROSS = [(1, 1), (3, 1), (2, 1)]
 INPUTS = (
     "zf",
     "zb",
@@ -526,23 +548,25 @@
     has_extra = extra_block(q)
     main, rest = f.base * LANES, (f.most - f.base) * LANES
 
-    def weight_copies(src_s, j, kinds):
+    def weight_copies(src_s, j, kinds, stage=None):
         start = first_block(j)
         at = pl.ds(pl.multiple_of(start * LANES, LANES), main)
         at2 = pl.ds(pl.multiple_of((start + f.base) * LANES, LANES), LANES)
         k = pl.ds(pl.multiple_of(src_s * LANES, LANES), LANES)
+        wide = R.wup.at[k, :] if stage is None else R.su.at[stage]
+        tall = R.wdn.at[:, k] if stage is None else R.sd.at[stage]
         out = []
         if "up" in kinds:
-            out.append((0, None, R.gate_w.at[:, at], R.wup.at[k, pl.ds(0, main)]))
-            out.append((1, None, R.value_w.at[:, at], R.wup.at[k, pl.ds(U, main)]))
+            out.append((0, None, R.gate_w.at[:, at], wide.at[:, pl.ds(0, main)]))
+            out.append((1, None, R.value_w.at[:, at], wide.at[:, pl.ds(U, main)]))
             if rest:
                 e = extra_block(j)
-                out.append((2, e, R.gate_w.at[:, at2], R.wup.at[k, pl.ds(main, LANES)]))
-                out.append((3, e, R.value_w.at[:, at2], R.wup.at[k, pl.ds(U + main, LANES)]))
+                out.append((2, e, R.gate_w.at[:, at2], wide.at[:, pl.ds(main, LANES)]))
+                out.append((3, e, R.value_w.at[:, at2], wide.at[:, pl.ds(U + main, LANES)]))
         if "down" in kinds:
-            out.append((4, None, R.down_w.at[at, :], R.wdn.at[pl.ds(0, main), k]))
+            out.append((4, None, R.down_w.at[at, :], tall.at[pl.ds(0, main), :]))
             if rest:
-                out.append((5, extra_block(j), R.down_w.at[at2, :], R.wdn.at[pl.ds(main, LANES), k]))
+                out.append((5, extra_block(j), R.down_w.at[at2, :], tall.at[pl.ds(main, LANES), :]))
         return out
 
     def own_weights(kinds):
@@ -553,24 +577,62 @@
             else:
                 pl.when(cond)(cp.start)
 
-    def send_weights(k, kinds):
-        j = lax.rem(q + k, Q)
-        for i, cond, src, dst in weight_copies(s, j, kinds):
-            go(remote(src, dst, R.w_s.at[k, i], R.w_r.at[q, i], {"sp": j * 2 + c, "tp": x}), cond)
-
-    def pass_weights(p, kinds):
-        ps = p * 2 + c
-        for i, cond, _, dst in weight_copies(ps, q, kinds):
-            cp = remote(dst, dst, R.w_s.at[0, i], R.w_r.at[p, i], to(c=1 - c))
+    def kin(dz, dy, sign=1):
+        return lax.rem(z + sign * dz + 4, 4) * 2 + (1 - y if dy else y)
+
+    def send_weights(classes, kinds):
+        for dz, dy in classes:
+            j = kin(dz, dy)
+            for i, cond, src, dst in weight_copies(s, j, kinds):
+                go(
+                    remote(src, dst, R.w_s.at[2 * dz + dy, i], R.w_r.at[q, i], {"sp": j * 2 + c, "tp": x}),
+                    cond,
+                )
+
+    def lend_weights(distances, kinds):
+        for dz in distances:
+            j = kin(dz, 1)
+            for i, cond, src, dst in weight_copies(s, j, kinds, dz - 1):
+                go(remote(src, dst, R.sy_s.at[dz, i], R.sy_r.at[dz, i], to(y=1 - y)), cond)
+
+    def arrived(copies, sems):
+        for i, cond, _, dst in copies:
+            cp = remote(dst, dst, R.w_s.at[0, i], sems.at[i], to(y=1 - y))
             if cond is None:
                 cp.wait_recv()
             else:
                 pl.when(cond)(cp.wait_recv)
-        k = pl.ds(pl.multiple_of(ps * LANES, LANES), LANES)
-        if "up" in kinds:
-            go(remote(R.wup.at[k, :], R.wup.at[k, :], R.f_s.at[p, 0], R.f_r.at[p, 0], to(c=1 - c)))
-        if "down" in kinds:
-            go(remote(R.wdn.at[:, k], R.wdn.at[:, k], R.f_s.at[p, 1], R.f_r.at[p, 1], to(c=1 - c)))
+
+    def relay_weights(distances, kinds):
+        peer = z * 2 + 1 - y
+        k = lane(peer * 2 + c)
+        for dz in distances:
+            j = kin(dz, 0)
+            arrived(weight_copies(s, j, kinds, dz - 1), R.sy_r.at[dz])
+            dev = {"sp": j * 2 + c, "tp": x}
+            if "up" in kinds:
+                go(remote(R.su.at[dz - 1], R.wup.at[k, :], R.w_s.at[2 * dz + 1, 0], R.w_r.at[peer, 0], dev))
+            if "down" in kinds:
+                go(remote(R.sd.at[dz - 1], R.wdn.at[:, k], R.w_s.at[2 * dz + 1, 4], R.w_r.at[peer, 4], dev))
+
+    def pass_weights(classes, kinds):
+        for dz, dy in classes:
+            p = kin(dz, dy, -1)
+            ps = p * 2 + c
+            k = lane(ps)
+            if dz and dy:
+                whole = []
+                if "up" in kinds:
+                    whole.append((0, None, None, R.wup.at[k, :]))
+                if "down" in kinds:
+                    whole.append((4, None, None, R.wdn.at[:, k]))
+                arrived(whole, R.w_r.at[p])
+            else:
+                arrived(weight_copies(ps, q, kinds), R.w_r.at[p])
+            if "up" in kinds:
+                go(remote(R.wup.at[k, :], R.wup.at[k, :], R.f_s.at[p, 0], R.f_r.at[p, 0], to(c=1 - c)))
+            if "down" in kinds:
+                go(remote(R.wdn.at[:, k], R.wdn.at[:, k], R.f_s.at[p, 1], R.f_r.at[p, 1], to(c=1 - c)))
 
     def wait_weights(p, kind):
         k = pl.ds(pl.multiple_of((p * 2 + 1 - c) * LANES, LANES), LANES)
@@ -622,6 +684,13 @@
             R.wup[:, main:U] = jnp.zeros((D, LANES), BF16)
             R.wup[:, U + main :] = jnp.zeros((D, LANES), BF16)
             R.wdn[main:U, :] = jnp.zeros((LANES, D), BF16)
+
+        for dz in range(1, g.z):
+            @pl.when(jnp.logical_not(extra_block(kin(dz, 0))))
+            def _(i=dz - 1):
+                R.su[i, :, main:U] = jnp.zeros((LANES, LANES), BF16)
+                R.su[i, :, U + main :] = jnp.zeros((LANES, LANES), BF16)
+                R.sd[i, main:U, :] = jnp.zeros((LANES, LANES), BF16)
 
     edge = jnp.zeros((2 * f.most, 8, LANES), F32)
     R.er[:, 0:8, :] = edge
@@ -636,21 +705,19 @@
     pl.semaphore_wait(barrier, Q + 1)
 
     ccol = lane(c)
-    O = f.quarter
-    starts = (2 * O + x * O, 0, O)
-    own_out = []
-    for i, (r, size) in enumerate(((starts[0], O), (0, 2 * O))):
-        at = pl.ds(pl.multiple_of(r, O), size)
-        cp = pltpu.make_async_copy(R.out_w.at[at, :], R.outm.at[z, y, at, ccol], R.loc_s.at[i])
-        cp.start()
-        own_out.append(cp)
+    O = f.piece
+    own_out = pltpu.make_async_copy(
+        R.out_w.at[pl.ds(pl.multiple_of(x * f.width, 16), f.width), :],
+        R.outm.at[z, y, :, ccol],
+        R.loc_s.at[0],
+    )
+    own_out.start()
     zg = []
-    for i, r in enumerate(starts):
-        at = pl.ds(pl.multiple_of(r, O), O)
+    for i in range(OUT_PIECES):
         zg.append(
             ZGather(
-                R.out_w.at[at, :],
-                lambda k, at=at: R.outm.at[k, y, at, ccol],
+                R.out_w.at[pl.ds(pl.multiple_of(x * f.width + i * O, 16), O), :],
+                lambda k, i=i: R.outm.at[k, y, pl.ds(i * O, O), ccol],
                 lambda j, i=i: R.oz_s.at[i, j],
                 lambda j, i=i: R.oz_r.at[i, j],
             )
@@ -658,21 +725,16 @@
         zg[-1].start()
 
     def out_y(i):
-        at = pl.ds(pl.multiple_of(starts[i], O), O)
-        src = R.outm.at[:, y, at, ccol]
+        src = R.outm.at[:, y, pl.ds(i * O, O), ccol]
         return remote(src, src, R.oy_s.at[i], R.oy_r.at[i], to(y=1 - y))
-
-    def out_x():
-        at = pl.ds(pl.multiple_of(starts[0], O), O)
-        src = R.outm.at[:, :, at, ccol]
-        return remote(src, src, R.ox_s.at[0], R.ox_r.at[0], to(x=1 - x))
 
     def out_c(i):
         src = R.outm.at[:, :, pl.ds(i * O, O), ccol]
         return remote(src, src, R.oc_s.at[i], R.oc_r.at[i], to(c=1 - c))
 
     own_weights(("up",))
-    send_weights(1, ("up",))
+    send_weights([(0, 1)], ("up",))
+    lend_weights([1], ("up",))
 
     L = f.length
     rows_i = lax.broadcasted_iota(jnp.int32, (L, L), 0)
@@ -720,10 +782,17 @@
     def hop(i, src, dst, dev):
         return go(remote(src, dst, R.st_s.at[i], R.st_r.at[i], dev))
 
+    out_ys, out_cs = {}, {}
+
+    def out_second(i):
+        zg[i].finish()
+        out_ys[i] = go(out_y(i))
+
+    def out_third(i):
+        out_ys[i].wait_recv()
+        out_cs[i] = go(out_c(i))
+
     step = hop(0, R.stb.at[1 - c], R.rc, to(c=1 - c))
-    for o in zg:
-        o.forward()
-    send_weights(2, ("up",))
     step.wait_recv()
     for hp in range(2):
         for d in range(2):
@@ -733,13 +802,8 @@
             both = jnp.where(ahead, ap, ao) * jnp.where(ahead, so, sp_) + jnp.where(ahead, sp_, so)
             put(R.ct, (hp, d), both, ao * ap)
     step = hop(1, R.ct.at[1 - y], R.ry, to(y=1 - y))
-    for cp in own_out:
-        cp.wait()
-    out_ys = []
-    for i, o in enumerate(zg):
-        o.finish()
-        out_ys.append(go(out_y(i)))
-    send_weights(7, ("up",))
+    zg[0].forward()
+    own_out.wait()
     step.wait_recv()
     for d in range(2):
         ahead = y == d
@@ -752,10 +816,11 @@
         zt = lax.rem(z + k, 4)
         src = R.pt.at[jnp.where(zt > z, 0, 1)]
         hops.append(go(remote(src, R.rz.at[z], R.sz_s.at[k - 1], R.sz_r.at[k - 1], to(z=zt))))
-    out_ys[0].wait_recv()
-    out_xs = go(out_x())
-    send_weights(6, ("up",))
-    send_weights(3, ("up",))
+    zg[1].forward()
+    out_second(0)
+    zg[2].forward()
+    zg[3].forward()
+    send_weights(STRAIGHT[:1], ("up",))
     for h_ in hops:
         h_.wait_recv()
 
@@ -773,12 +838,9 @@
         R.ce[y, d] = jnp.where(y == d, e, ap * e + sp_).astype(BF16)
         R.yb[d] = jnp.where(y == d, ao * e + so, e).astype(BF16)
     step = hop(2, R.yb, R.ce.at[y], to(y=1 - y))
-    out_cs = []
-    for i in (1, 2):
-        out_ys[i].wait_recv()
-        out_cs.append(go(out_c(i - 1)))
-    send_weights(5, ("up",))
-    send_weights(4, ("up",))
+    out_second(1)
+    out_second(2)
+    send_weights(STRAIGHT[1:2], ("up",))
     step.wait_recv()
     for hp in range(2):
         for d in range(2):
@@ -788,12 +850,15 @@
             R.ent[c, hp, d] = jnp.where(c == d, e, ap * e + sp_).astype(BF16)
             R.cb[hp, d] = jnp.where(c == d, ao * e + so, e).astype(BF16)
     step = hop(3, R.cb, R.ent.at[c], to(c=1 - c))
-    out_xs.wait_recv()
-    for i in (2, 3):
-        out_cs.append(go(out_c(i)))
+    out_second(3)
+    out_third(0)
+    lend_weights([3, 2], ("up",))
+    send_weights(STRAIGHT[2:], ("up",))
+    lend_weights([1, 3, 2], ("down",))
+    send_weights([(0, 1)], ("down",))
     step.wait_recv()
 
-    def finish(half, write):
+    for first, half in enumerate((1 - x, x)):
         at_rows = pl.ds(pl.multiple_of(half * H, H), H)
         for h in range(f.heads):
             at = slice(h * W, (h + 1) * W)
@@ -802,32 +867,32 @@
                 total += dot(R.carry[d, at_rows, at], R.ent[h // 2, h % 2, d], ((1,), (1,)))
             mean = jnp.mean(total * total, axis=-1, keepdims=True)
             gate = R.og[at_rows, at].astype(F32)
-            write(
-                at,
-                (
-                    total * lax.rsqrt(mean + EPSILON) * R.hscale[...] * (gate * jax.nn.sigmoid(gate))
-                ).astype(BF16),
-            )
-
-    def write_peer(at, value):
-        R.gb[:, at] = value
-
-    def write_own(at, value):
-        R.sw[x, :, at] = value
-
-    finish(1 - x, write_peer)
-    step = hop(4, R.gb, R.sw.at[x], to(x=1 - x))
-    finish(x, write_own)
-    for o in out_cs:
-        o.wait_recv()
-    step.wait_recv()
-    square = jnp.zeros((H, 1), F32)
+            R.gb[first * H : (first + 1) * H, at] = (
+                total * lax.rsqrt(mean + EPSILON) * R.hscale[...] * (gate * jax.nn.sigmoid(gate))
+            ).astype(BF16)
+    for i in range(1, OUT_PIECES):
+        out_third(i)
+    for i in range(OUT_PIECES):
+        out_cs[i].wait_recv()
+
     width = g.c * LANES
+    swaps = []
     for p in range(Q):
         at = slice(p * width, (p + 1) * width)
-        total = R.res[:, at].astype(F32)
-        for t in range(2):
-            total += dot(R.sw[t], R.outm[p // 2, p % 2, t * f.width : (t + 1) * f.width], ((1,), (0,)))
+        total = dot(R.gb[...], R.outm[p // 2, p % 2], ((1,), (0,)))
+        R.xb[:, at] = total[:H].astype(BF16)
+        R.after[:, at] = R.res[:, at].astype(F32) + total[H:]
+        if p % 2:
+            i = p // 2
+            two = pl.ds(2 * i * width, 2 * width)
+            swaps.append(
+                go(remote(R.xb.at[:, two], R.xr.at[:, two], R.xs_s.at[i], R.xs_r.at[i], to(x=1 - x)))
+            )
+    square = jnp.zeros((H, 1), F32)
+    for i, swap in enumerate(swaps):
+        at = slice(2 * i * width, 2 * (i + 1) * width)
+        swap.wait_recv()
+        total = R.after[:, at] + R.xr[:, at].astype(F32)
         R.after[:, at] = total
         square += jnp.sum(total * total, axis=-1, keepdims=True)
     scale = lax.rsqrt(square / D + EPSILON)
@@ -835,13 +900,14 @@
         at = slice(p * width, (p + 1) * width)
         R.tok[z, y, x, :, at] = (R.after[:, at] * scale * R.pscale[:, at]).astype(BF16)
 
-    n, S = 2 * SLICES, f.step
+    n = len(f.gather)
+    G = n // 2
 
     def cols(k):
-        return slice(k * S, (k + 1) * S)
+        return slice(f.gather[k][0], sum(f.gather[k]))
 
     def cds(k):
-        return pl.ds(k * S, S)
+        return pl.ds(*f.gather[k])
 
     ag = []
     for k in range(n):
@@ -855,59 +921,63 @@
         )
 
     def pair(t):
-        return (t, t + SLICES)
+        return (t, t + G)
 
     def second(k):
         src = R.tok.at[:, y, x, :, cds(k)]
-        dev = to(x=1 - x) if k < SLICES else to(y=1 - y)
+        dev = to(x=1 - x) if k < G else to(y=1 - y)
         return remote(src, src, R.a2_s.at[k], R.a2_r.at[k], dev)
 
     def third(k):
-        if k < SLICES:
+        if k < G:
             src, dev = R.tok.at[:, y, :, :, cds(k)], to(y=1 - y)
         else:
             src, dev = R.tok.at[:, :, x, :, cds(k)], to(x=1 - x)
         return remote(src, src, R.a3_s.at[k], R.a3_r.at[k], dev)
 
-    def up(k, first):
-        wait_weights(k, 0)
+    def up(t, first):
         tall = g.y * g.x * H
 
         def body(i, _):
             at = pl.ds(pl.multiple_of(i * tall, tall), tall)
-            value = dot(R.tok[i, :, :, :, cols(k)].reshape(tall, S), R.wup[cols(k), :], ((1,), (0,)))
+            value = 0.0
+            for k in pair(t):
+                rows = R.tok[i, :, :, :, cols(k)].reshape(tall, f.gather[k][1])
+                value += dot(rows, R.wup[cols(k), :], ((1,), (0,)))
             R.acc[at, :] = value if first else R.acc[at, :] + value
             return 0
 
         lax.fori_loop(0, g.z, body, 0)
 
-    for t in range(SLICES):
+    for t in range(G):
         for k in pair(t):
             ag[k].start()
     own_weights(("down",))
+    pass_weights(NEAR + STRAIGHT, ("up",))
     flying = {}
-    for t in range(SLICES + 3):
-        if t < SLICES:
+    for t in range(G + 2):
+        if t < G:
             for k in pair(t):
                 ag[k].forward()
-        if 0 <= t - 1 < SLICES:
+            if t == G - 1:
+                relay_weights([1, 3, 2], ("up",))
+                send_weights(STRAIGHT, ("down",))
+                relay_weights([1, 3, 2], ("down",))
+        if 0 <= t - 1 < G:
             for k in pair(t - 1):
                 ag[k].finish()
                 flying[2, k] = go(second(k))
-        if t < SLICES:
-            pass_weights(2 * t, ("up",))
-            pass_weights(2 * t + 1, ("up",))
-            send_weights(2 * t + 1, ("down",))
-            if 2 * t + 2 < Q:
-                send_weights(2 * t + 2, ("down",))
-        if 0 <= t - 2 < SLICES:
+        if 0 <= t - 2 < G:
             for k in pair(t - 2):
                 flying[2, k].wait_recv()
                 flying[3, k] = go(third(k))
-        if 0 <= t - 3 < SLICES:
-            for k in pair(t - 3):
-                flying[3, k].wait_recv()
-                up(k, k == 0)
+    pass_weights(CROSS, ("up",))
+    for p in range(Q):
+        wait_weights(p, 0)
+    for t in range(G):
+        for k in pair(t):
+            flying[3, k].wait_recv()
+        up(t, t == 0)
 
     for i in range(Q):
         for e, row in enumerate((i * L, (i + 1) * L - 1)):
@@ -917,8 +987,7 @@
     edges = go(
         remote(R.ed, R.er.at[:, pl.ds(8, 2 * Q), :], R.ed_s.at[0], R.ed_r.at[0], to(c=1 - c))
     )
-    for p in range(Q):
-        pass_weights(p, ("down",))
+    pass_weights(NEAR + STRAIGHT + CROSS, ("down",))
     edges.wait_recv()
     top = lax.broadcasted_iota(jnp.int32, (L, LANES), 0)
 
@@ -946,37 +1015,49 @@
     for p in range(Q):
         wait_weights(p, 1)
 
+    n = len(f.reduce)
+    G = n // 2
+
+    def cols(k):
+        return slice(f.reduce[k][0], sum(f.reduce[k]))
+
+    def cds(k):
+        return pl.ds(*f.reduce[k])
+
+    def pair(t):
+        return (t, t + G)
+
     def down(k):
         tall = g.y * g.x * H
 
         def body(i, _):
             at = pl.ds(pl.multiple_of(i * tall, tall), tall)
             value = dot(R.hid[at, :], R.wdn[:, cols(k)], ((1,), (0,)))
-            R.part[i, :, :, :, cols(k)] = value.astype(BF16).reshape(g.y, g.x, H, S)
+            R.part[i, :, :, :, cols(k)] = value.astype(BF16).reshape(g.y, g.x, H, f.reduce[k][1])
             return 0
 
         lax.fori_loop(0, g.z, body, 0)
 
     def first_sum(k):
-        if k < SLICES:
+        if k < G:
             src, dev = R.part.at[:, 1 - y, :, :, cds(k)], to(y=1 - y)
         else:
             src, dev = R.part.at[:, :, 1 - x, :, cds(k)], to(x=1 - x)
-        return remote(src, R.r1.at[k], R.r1_s.at[k], R.r1_r.at[k], dev)
+        return remote(src, R.r1.at[:, :, :, cds(k)], R.r1_s.at[k], R.r1_r.at[k], dev)
 
     def second_sum(k):
-        if k < SLICES:
+        if k < G:
             src, dev = R.part.at[:, y, 1 - x, :, cds(k)], to(x=1 - x)
         else:
             src, dev = R.part.at[:, 1 - y, x, :, cds(k)], to(y=1 - y)
-        return remote(src, R.r2.at[k], R.r2_s.at[k], R.r2_r.at[k], dev)
+        return remote(src, R.r2.at[:, :, cds(k)], R.r2_s.at[k], R.r2_r.at[k], dev)
 
     def add_first(k):
         def body(i, _):
             zi, j = i // 2, lax.rem(i, 2)
-            at = (zi, y, j) if k < SLICES else (zi, j, x)
+            at = (zi, y, j) if k < G else (zi, j, x)
             at = at + (slice(None), cols(k))
-            R.part[at] = (R.part[at].astype(F32) + R.r1[k, zi, j].astype(F32)).astype(BF16)
+            R.part[at] = (R.part[at].astype(F32) + R.r1[zi, j, :, cols(k)].astype(F32)).astype(BF16)
             return 0
 
         lax.fori_loop(0, 2 * g.z, body, 0)
@@ -984,7 +1065,7 @@
     def add_second(k):
         def body(i, _):
             at = (i, y, x, slice(None), cols(k))
-            R.part[at] = (R.part[at].astype(F32) + R.r2[k, i].astype(F32)).astype(BF16)
+            R.part[at] = (R.part[at].astype(F32) + R.r2[i, :, cols(k)].astype(F32)).astype(BF16)
             return 0
 
         lax.fori_loop(0, g.z, body, 0)
@@ -995,32 +1076,48 @@
             zt = lax.rem(z + j, 4)
             src = R.part.at[zt, y, x, :, cds(k)]
             sums.append(
-                go(remote(src, R.r3.at[k, j - 1], R.r3_s.at[k, j - 1], R.r3_r.at[k, j - 1], to(z=zt)))
+                go(remote(src, R.r3.at[j - 1, :, cds(k)], R.r3_s.at[k, j - 1], R.r3_r.at[k, j - 1], to(z=zt)))
             )
         return sums
 
-    for t in range(SLICES):
+    def stage1(t):
+        for k in pair(t):
+            flying[4, k] = go(first_sum(k))
+
+    def stage2(t):
+        for k in pair(t):
+            flying[4, k].wait_recv()
+            add_first(k)
+            flying[5, k] = go(second_sum(k))
+
+    def stage3(t):
+        for k in pair(t):
+            flying[5, k].wait_recv()
+            add_second(k)
+            flying[6, k] = last_sums(k)
+
+    def stage4(t):
+        for k in pair(t):
+            total = R.after[:, cols(k)] + R.part[z, y, x, :, cols(k)].astype(F32)
+            for j, cp in enumerate(flying[6, k]):
+                cp.wait_recv()
+                total += R.r3[j, :, cols(k)].astype(F32)
+            R.out[:, cols(k)] = total.astype(BF16)
+
+    for t in range(G):
         for k in pair(t):
             down(k)
-            flying[4, k] = go(first_sum(k))
-    for t in range(1, SLICES + 3):
-        if t - 1 < SLICES:
-            for k in pair(t - 1):
-                flying[4, k].wait_recv()
-                add_first(k)
-                flying[5, k] = go(second_sum(k))
-        if 0 <= t - 2 < SLICES:
-            for k in pair(t - 2):
-                flying[5, k].wait_recv()
-                add_second(k)
-                flying[6, k] = last_sums(k)
-        if 0 <= t - 3 < SLICES:
-            for k in pair(t - 3):
-                total = R.after[:, cols(k)] + R.part[z, y, x, :, cols(k)].astype(F32)
-                for j, cp in enumerate(flying[6, k]):
-                    cp.wait_recv()
-                    total += R.r3[k, j].astype(F32)
-                R.out[:, cols(k)] = total.astype(BF16)
+            if t < 2:
+                flying[4, k] = go(first_sum(k))
+    for t in range(G + 2):
+        if t < G:
+            stage2(t)
+        if t + 2 < G:
+            stage1(t + 2)
+        if 0 <= t - 1 < G:
+            stage3(t - 1)
+        if 0 <= t - 2 < G:
+            stage4(t - 2)
     for cond, cp in drains:
         if cond is None:
             cp.wait_send()

time: 176 us -> 150 us (0.85)
  Pallas kernels: 173 us -> 147 us
    pallas_call x1, Pallas kernels: 173 us -> 147 us  [fused(): pl.pallas_call(functools.partial(fused_kernel, f, list(scratch)), out_sha...]
where the time goes in v2:
time: 150 us
  Pallas kernels  147 us (98%)
  local copies, waits for them, and re-layouts  3.15 us (2%)
    pallas_call x1, Pallas kernels, fused(): pl.pallas_call(functools.partial(fused_kernel, f, list(scratch)), out_sha...  147 us
    unnamed x2, local copies, waits for them, and re-layouts  3.15 us

profile of v2, /device:TPU:0, one launch (start us, length us, event | category | flops | bytes accessed | tf_op | source)
XLA Modules:
  0.0 149.8 jit_solution(6113559236473747163)
XLA Ops:
  0.0 1.5 copy.17.refs_6_
  1.5 146.7 %shard_map.154 = bf16[64,2048]{1,0:T(8,128)(2,1)} custom-call(bf16[128,512]{1,0:T(8,128)(2,1)} %refs_0_.1, bf16[128,512]{1,0:T(8,128)(2,1)} %refs_1_.1, bf16[128,512]{1,0:T(8,128)(2,1)} %refs_2_.1, bf16[128,512]{1,0:T(8,128)(2,1)} %refs_3_.1, bf16[128,512]{1,0:T(8,128)(2,1)} %refs_4_.1, f32[2,512]{1,0:T(2,128)} %refs_5_.1, f32[2,128,4]{2,1,0:T(8,128)} %copy.17.refs_6_, ...), custom_call_target="tpu_custom_call" | custom-call | tf_op jit(solution)/shard_map/pallas_call | solution.py:1132
  148.2 1.7 %copy.19 = bf16[64,2048]{1,0:T(8,128)(2,1)} copy(bf16[64,2048]{1,0:T(8,128)(2,1)} %shard_map.154) | data formatting | bytes 524288

commit v3 on v2

--- a/solution.py
+++ b/solution.py
@@ -383,8 +383,10 @@
 
 LANES = 128
 PAD_ROWS = 16
-GATHER_WIDTHS = (2, 2, 2, 2)
-REDUCE_WIDTHS = (3, 2, 2, 1)
+GATHER_WIDTHS = ((1, 1, 2, 1, 1), (1, 2, 3, 2, 2))
+REDUCE_WIDTHS = ((1, 2, 2, 1, 1), (1, 2, 2, 1, 1))
+SIDE = 1
+LEND = 2
 OUT_PIECES = 4
 
 
@@ -402,15 +404,15 @@
         self.shards = self.quads * grid.x
         self.own = self.shards * self.rows
         self.gather = self.split(GATHER_WIDTHS)
-        self.reduce = self.split(REDUCE_WIDTHS)
+        self.reduce = self.split(REDUCE_WIDTHS, 2 * SIDE)
+        self.side = (depth - sum(self.reduce[-1])) // 2
         self.piece = width // OUT_PIECES
 
-    def split(self, widths):
-        unit = self.depth // 2 // sum(widths)
-        out = []
-        for color in range(2):
-            first = color * (self.depth // 2)
-            for w in widths:
+    def split(self, widths, spare=0):
+        unit = self.depth // (sum(map(sum, widths)) + spare)
+        out, first = [], 0
+        for color in widths:
+            for w in color:
                 out.append((first, w * unit))
                 first += w * unit
         return out
@@ -424,8 +426,8 @@
             and units // LANES >= grid.z * grid.y
             and length % (16 * grid.x) == 0
             and depth == out_depth == grid.sp * LANES
-            and depth % (2 * LANES * sum(GATHER_WIDTHS)) == 0
-            and depth % (2 * LANES * sum(REDUCE_WIDTHS)) == 0
+            and depth % (LANES * sum(map(sum, GATHER_WIDTHS))) == 0
+            and depth % (LANES * (sum(map(sum, REDUCE_WIDTHS)) + 2 * SIDE)) == 0
             and width % (16 * OUT_PIECES) == 0
         )
 
@@ -463,6 +465,19 @@
             r1=pltpu.VMEM((g.z, 2, self.rows, self.depth), BF16),
             r2=pltpu.VMEM((g.z, self.rows, self.depth), BF16),
             r3=pltpu.VMEM((g.z - 1, self.rows, self.depth), BF16),
+            c1=pltpu.VMEM((g.z - 1, g.y, g.x, self.rows, 2 * self.side), BF16),
+            c2=pltpu.VMEM((2, 2, self.rows, self.side), BF16),
+            c3=pltpu.VMEM((2, self.rows, self.side), BF16),
+            c1_s=dma((1,)), c1_r=dma((1,)),
+            c2_s=dma((2,)), c2_r=dma((2,)),
+            c3_s=dma((2,)), c3_r=dma((2,)),
+            zf=pltpu.VMEM((self.length, self.width), BF16),
+            zb=pltpu.VMEM((self.length, self.width), BF16),
+            val=pltpu.VMEM((self.length, self.width), BF16),
+            qry=pltpu.VMEM((self.length, self.width), BF16),
+            og=pltpu.VMEM((self.length, self.width), BF16),
+            res=pltpu.VMEM((self.rows, self.depth), BF16),
+            in_s=dma((6,)),
             loc_s=dma((1,)),
             oz_s=dma((OUT_PIECES, 4)), oz_r=dma((OUT_PIECES, 4)),
             oy_s=dma((OUT_PIECES,)), oy_r=dma((OUT_PIECES,)),
@@ -470,18 +485,20 @@
             xs_s=dma((4,)), xs_r=dma((4,)),
             su=pltpu.VMEM((g.z - 1, LANES, 2 * self.unit), BF16),
             sd=pltpu.VMEM((g.z - 1, self.unit, LANES), BF16),
-            sy_s=dma((g.z, 6)), sy_r=dma((g.z, 6)),
-            w_s=dma((self.quads, 6)), w_r=dma((self.quads, 6)),
+            sy_s=dma((g.z - 1, 2)), sy_r=dma((g.z - 1, 2)),
+            w_s=dma((self.quads, 2)), w_r=dma((self.quads, 2)),
             f_s=dma((self.quads, 2)), f_r=dma((self.quads, 2)),
             st_s=dma((4,)), st_r=dma((4,)),
-            sz_s=dma((3,)), sz_r=dma((3,)),
+            sz_s=dma((1,)), sz_r=dma((1,)),
             az_s=dma((n, 4)), az_r=dma((n, 4)),
+            ao_s=dma((2,)), ao_r=dma((2,)),
+            at_s=dma((2, 2)), at_r=dma((2, 2)),
             a2_s=dma((n,)), a2_r=dma((n,)),
             a3_s=dma((n,)), a3_r=dma((n,)),
             ed_s=dma((1,)), ed_r=dma((1,)),
             r1_s=dma((m,)), r1_r=dma((m,)),
             r2_s=dma((m,)), r2_r=dma((m,)),
-            r3_s=dma((m, 3)), r3_r=dma((m, 3)),
+            r3_s=dma((m,)), r3_r=dma((m,)),
         )
 
 
@@ -489,15 +506,15 @@
 STRAIGHT = [(1, 0), (3, 0), (2, 0)]
 CROSS = [(1, 1), (3, 1), (2, 1)]
 INPUTS = (
-    "zf",
-    "zb",
-    "val",
-    "qry",
-    "og",
+    "zf_in",
+    "zb_in",
+    "val_in",
+    "qry_in",
+    "og_in",
     "floor",
     "extra",
     "hscale",
-    "res",
+    "res_in",
     "pscale",
     "gtaps",
     "vtaps",
@@ -527,12 +544,10 @@
             src_ref=src, dst_ref=dst, send_sem=ss, recv_sem=rs, device_id=dev, device_id_type=MESH
         )
 
-    def go(cp, cond=None):
-        if cond is None:
+    def go(cp, start=True):
+        if start:
             cp.start()
-        else:
-            pl.when(cond)(cp.start)
-        drains.append((cond, cp))
+        drains.append((None, cp))
         return cp
 
     def lane(i):
@@ -548,91 +563,110 @@
     has_extra = extra_block(q)
     main, rest = f.base * LANES, (f.most - f.base) * LANES
 
-    def weight_copies(src_s, j, kinds, stage=None):
+    def spots(src_s, stage):
+        if stage is None:
+            k = lane(src_s)
+            return R.wup.at[k, :], R.wdn.at[:, k]
+        return R.su.at[stage], R.sd.at[stage]
+
+    def weight_copies(src_s, j, kind, stage=None):
         start = first_block(j)
         at = pl.ds(pl.multiple_of(start * LANES, LANES), main)
         at2 = pl.ds(pl.multiple_of((start + f.base) * LANES, LANES), LANES)
-        k = pl.ds(pl.multiple_of(src_s * LANES, LANES), LANES)
-        wide = R.wup.at[k, :] if stage is None else R.su.at[stage]
-        tall = R.wdn.at[:, k] if stage is None else R.sd.at[stage]
-        out = []
-        if "up" in kinds:
-            out.append((0, None, R.gate_w.at[:, at], wide.at[:, pl.ds(0, main)]))
-            out.append((1, None, R.value_w.at[:, at], wide.at[:, pl.ds(U, main)]))
+        dst = spots(src_s, stage)[kind]
+        e = extra_block(j)
+        if kind:
+            out = [(None, R.down_w.at[at, :], dst.at[pl.ds(0, main), :])]
             if rest:
-                e = extra_block(j)
-                out.append((2, e, R.gate_w.at[:, at2], wide.at[:, pl.ds(main, LANES)]))
-                out.append((3, e, R.value_w.at[:, at2], wide.at[:, pl.ds(U + main, LANES)]))
-        if "down" in kinds:
-            out.append((4, None, R.down_w.at[at, :], tall.at[pl.ds(0, main), :]))
-            if rest:
-                out.append((5, extra_block(j), R.down_w.at[at2, :], tall.at[pl.ds(main, LANES), :]))
+                out.append((e, R.down_w.at[at2, :], dst.at[pl.ds(main, LANES), :]))
+            return out
+        out = [
+            (None, R.gate_w.at[:, at], dst.at[:, pl.ds(0, main)]),
+            (None, R.value_w.at[:, at], dst.at[:, pl.ds(U, main)]),
+        ]
+        if rest:
+            out.append((e, R.gate_w.at[:, at2], dst.at[:, pl.ds(main, LANES)]))
+            out.append((e, R.value_w.at[:, at2], dst.at[:, pl.ds(U + main, LANES)]))
         return out
 
-    def own_weights(kinds):
-        for i, cond, src, dst in weight_copies(s, q, kinds):
-            cp = pltpu.make_async_copy(src, dst, R.w_r.at[q, i])
-            if cond is None:
-                cp.start()
-            else:
-                pl.when(cond)(cp.start)
+    def when(cond, act):
+        if cond is None:
+            act()
+        else:
+            pl.when(cond)(act)
+
+    def totals(dst, kind, extra):
+        less = dst.at[pl.ds(0, main), :] if kind else dst.at[:, pl.ds(0, 2 * main)]
+        if not rest:
+            return [(None, dst)]
+        return [(extra, dst), (jnp.logical_not(extra), less)]
+
+    def arrived(dst, kind, extra, sem):
+        for cond, ref in totals(dst, kind, extra):
+            when(cond, remote(ref, ref, R.w_s.at[0, kind], sem, to(y=1 - y)).wait_recv)
+
+    def sent(dst, kind, extra, sem):
+        for cond, ref in totals(dst, kind, extra):
+            drains.append((cond, remote(ref, ref, sem, R.w_r.at[0, kind], to(y=1 - y))))
+
+    def own_weights(kind):
+        for cond, src, dst in weight_copies(s, q, kind):
+            when(cond, pltpu.make_async_copy(src, dst, R.w_r.at[q, kind]).start)
 
     def kin(dz, dy, sign=1):
         return lax.rem(z + sign * dz + 4, 4) * 2 + (1 - y if dy else y)
 
-    def send_weights(classes, kinds):
+    def send_weights(classes, kind):
         for dz, dy in classes:
             j = kin(dz, dy)
-            for i, cond, src, dst in weight_copies(s, j, kinds):
-                go(
-                    remote(src, dst, R.w_s.at[2 * dz + dy, i], R.w_r.at[q, i], {"sp": j * 2 + c, "tp": x}),
-                    cond,
-                )
-
-    def lend_weights(distances, kinds):
+            sem = R.w_s.at[2 * dz + dy, kind]
+            for cond, src, dst in weight_copies(s, j, kind):
+                when(cond, remote(src, dst, sem, R.w_r.at[q, kind], {"sp": j * 2 + c, "tp": x}).start)
+            sent(spots(s, None)[kind], kind, extra_block(j), sem)
+
+    def lend_weights(distances, kind):
         for dz in distances:
             j = kin(dz, 1)
-            for i, cond, src, dst in weight_copies(s, j, kinds, dz - 1):
-                go(remote(src, dst, R.sy_s.at[dz, i], R.sy_r.at[dz, i], to(y=1 - y)), cond)
-
-    def arrived(copies, sems):
-        for i, cond, _, dst in copies:
-            cp = remote(dst, dst, R.w_s.at[0, i], sems.at[i], to(y=1 - y))
-            if cond is None:
-                cp.wait_recv()
-            else:
-                pl.when(cond)(cp.wait_recv)
-
-    def relay_weights(distances, kinds):
+            sem = R.sy_s.at[dz - 1, kind]
+            for cond, src, dst in weight_copies(s, j, kind, dz - 1):
+                when(cond, remote(src, dst, sem, R.sy_r.at[dz - 1, kind], to(y=1 - y)).start)
+            sent(spots(s, None)[kind], kind, extra_block(j), sem)
+
+    def relay_weights(distances, kind):
         peer = z * 2 + 1 - y
-        k = lane(peer * 2 + c)
+        goal = spots(peer * 2 + c, None)[kind]
         for dz in distances:
             j = kin(dz, 0)
-            arrived(weight_copies(s, j, kinds, dz - 1), R.sy_r.at[dz])
+            extra = extra_block(j)
+            held = spots(None, dz - 1)[kind]
+            arrived(held, kind, extra, R.sy_r.at[dz - 1, kind])
             dev = {"sp": j * 2 + c, "tp": x}
-            if "up" in kinds:
-                go(remote(R.su.at[dz - 1], R.wup.at[k, :], R.w_s.at[2 * dz + 1, 0], R.w_r.at[peer, 0], dev))
-            if "down" in kinds:
-                go(remote(R.sd.at[dz - 1], R.wdn.at[:, k], R.w_s.at[2 * dz + 1, 4], R.w_r.at[peer, 4], dev))
-
-    def pass_weights(classes, kinds):
+            sem = R.w_s.at[2 * dz + 1, kind]
+            if kind:
+                parts = [pl.ds(0, main)]
+                pick = lambda ref, part: ref.at[part, :]
+            else:
+                parts = [pl.ds(0, main), pl.ds(U, main)]
+                pick = lambda ref, part: ref.at[:, part]
+            few = [
+                remote(pick(held, part), pick(goal, part), sem, R.w_r.at[peer, kind], dev)
+                for part in parts
+            ]
+            full = remote(held, goal, sem, R.w_r.at[peer, kind], dev)
+            if rest:
+                pl.when(extra)(full.start)
+                for cp in few:
+                    pl.when(jnp.logical_not(extra))(cp.start)
+            else:
+                full.start()
+            sent(held, kind, extra, sem)
+
+    def pass_weights(classes, kind):
         for dz, dy in classes:
             p = kin(dz, dy, -1)
-            ps = p * 2 + c
-            k = lane(ps)
-            if dz and dy:
-                whole = []
-                if "up" in kinds:
-                    whole.append((0, None, None, R.wup.at[k, :]))
-                if "down" in kinds:
-                    whole.append((4, None, None, R.wdn.at[:, k]))
-                arrived(whole, R.w_r.at[p])
-            else:
-                arrived(weight_copies(ps, q, kinds), R.w_r.at[p])
-            if "up" in kinds:
-                go(remote(R.wup.at[k, :], R.wup.at[k, :], R.f_s.at[p, 0], R.f_r.at[p, 0], to(c=1 - c)))
-            if "down" in kinds:
-                go(remote(R.wdn.at[:, k], R.wdn.at[:, k], R.f_s.at[p, 1], R.f_r.at[p, 1], to(c=1 - c)))
+            ref = spots(p * 2 + c, None)[kind]
+            arrived(ref, kind, has_extra, R.w_r.at[p, kind])
+            go(remote(ref, ref, R.f_s.at[p, kind], R.f_r.at[p, kind], to(c=1 - c)))
 
     def wait_weights(p, kind):
         k = pl.ds(pl.multiple_of((p * 2 + 1 - c) * LANES, LANES), LANES)
@@ -678,19 +712,27 @@
                 for k in range(3):
                     self.arrive(jnp.where(z == 0, 1 + k, k))
 
+    loads = [
+        pltpu.make_async_copy(src, dst, R.in_s.at[i])
+        for i, (src, dst) in enumerate(
+            (
+                (R.zf_in, R.zf),
+                (R.zb_in, R.zb),
+                (R.val_in, R.val),
+                (R.qry_in, R.qry),
+                (R.og_in, R.og),
+                (R.res_in, R.res),
+            )
+        )
+    ]
+    for cp in loads:
+        cp.start()
     if rest:
         @pl.when(jnp.logical_not(has_extra))
         def _():
             R.wup[:, main:U] = jnp.zeros((D, LANES), BF16)
             R.wup[:, U + main :] = jnp.zeros((D, LANES), BF16)
             R.wdn[main:U, :] = jnp.zeros((LANES, D), BF16)
-
-        for dz in range(1, g.z):
-            @pl.when(jnp.logical_not(extra_block(kin(dz, 0))))
-            def _(i=dz - 1):
-                R.su[i, :, main:U] = jnp.zeros((LANES, LANES), BF16)
-                R.su[i, :, U + main :] = jnp.zeros((LANES, LANES), BF16)
-                R.sd[i, main:U, :] = jnp.zeros((LANES, LANES), BF16)
 
     edge = jnp.zeros((2 * f.most, 8, LANES), F32)
     R.er[:, 0:8, :] = edge
@@ -732,14 +774,16 @@
         src = R.outm.at[:, :, pl.ds(i * O, O), ccol]
         return remote(src, src, R.oc_s.at[i], R.oc_r.at[i], to(c=1 - c))
 
-    own_weights(("up",))
-    send_weights([(0, 1)], ("up",))
-    lend_weights([1], ("up",))
-
+    own_weights(0)
+    send_weights([(0, 1)], 0)
+
+    for cp in loads:
+        cp.wait()
     L = f.length
     rows_i = lax.broadcasted_iota(jnp.int32, (L, L), 0)
     cols_i = lax.broadcasted_iota(jnp.int32, (L, L), 1)
     middle = L // 2
+    extra = [jnp.transpose(R.extra[d]) for d in range(2)]
     for h in range(f.heads):
         at = slice(h * W, (h + 1) * W)
         values = R.val[:, at]
@@ -751,7 +795,7 @@
             pre = z_ref[:, at].astype(F32)
             floor = R.floor[d : d + 1, at]
             span = 1.0 - floor
-            logf = jnp.log(floor + span * jax.nn.sigmoid(pre)) + R.extra[d, :, h : h + 1]
+            logf = jnp.log(floor + span * jax.nn.sigmoid(pre)) + extra[d][:, h : h + 1]
             key = span * jax.nn.sigmoid(-pre)
             running = dot(jnp.where(mask, 1.0, 0.0), logf, ((1,), (0,)), lax.Precision.HIGHEST)
             last = L - 1 if d == 0 else 0
@@ -815,12 +859,15 @@
     for k in range(1, 4):
         zt = lax.rem(z + k, 4)
         src = R.pt.at[jnp.where(zt > z, 0, 1)]
-        hops.append(go(remote(src, R.rz.at[z], R.sz_s.at[k - 1], R.sz_r.at[k - 1], to(z=zt))))
+        remote(src, R.rz.at[z], R.sz_s.at[0], R.sz_r.at[0], to(z=zt)).start()
+    three = R.rz.at[pl.ds(0, 3)]
+    hops = [go(remote(three, three, R.sz_s.at[0], R.sz_r.at[0], to(y=1 - y)), False)]
     zg[1].forward()
     out_second(0)
     zg[2].forward()
+    out_second(1)
     zg[3].forward()
-    send_weights(STRAIGHT[:1], ("up",))
+    send_weights(STRAIGHT, 0)
     for h_ in hops:
         h_.wait_recv()
 
@@ -838,9 +885,8 @@
         R.ce[y, d] = jnp.where(y == d, e, ap * e + sp_).astype(BF16)
         R.yb[d] = jnp.where(y == d, ao * e + so, e).astype(BF16)
     step = hop(2, R.yb, R.ce.at[y], to(y=1 - y))
-    out_second(1)
     out_second(2)
-    send_weights(STRAIGHT[1:2], ("up",))
+    out_second(3)
     step.wait_recv()
     for hp in range(2):
         for d in range(2):
@@ -850,12 +896,8 @@
             R.ent[c, hp, d] = jnp.where(c == d, e, ap * e + sp_).astype(BF16)
             R.cb[hp, d] = jnp.where(c == d, ao * e + so, e).astype(BF16)
     step = hop(3, R.cb, R.ent.at[c], to(c=1 - c))
-    out_second(3)
     out_third(0)
-    lend_weights([3, 2], ("up",))
-    send_weights(STRAIGHT[2:], ("up",))
-    lend_weights([1, 3, 2], ("down",))
-    send_weights([(0, 1)], ("down",))
+    lend_weights([1, 3, 2], 0)
     step.wait_recv()
 
     for first, half in enumerate((1 - x, x)):
@@ -892,6 +934,8 @@
     for i, swap in enumerate(swaps):
         at = slice(2 * i * width, 2 * (i + 1) * width)
         swap.wait_recv()
+        if i == 1:
+            relay_weights([1], 0)
         total = R.after[:, at] + R.xr[:, at].astype(F32)
         R.after[:, at] = total
         square += jnp.sum(total * total, axis=-1, keepdims=True)
@@ -923,17 +967,44 @@
     def pair(t):
         return (t, t + G)
 
+    spans = ((0, f.gather[G][0]), (f.gather[G][0], D - f.gather[G][0]))
+
+    def second_own(color):
+        src = R.tok.at[z, y, x, :, pl.ds(*spans[color])]
+        dev = to(y=1 - y) if color else to(x=1 - x)
+        return remote(src, src, R.ao_s.at[color], R.ao_r.at[color], dev)
+
     def second(k):
-        src = R.tok.at[:, y, x, :, cds(k)]
         dev = to(x=1 - x) if k < G else to(y=1 - y)
-        return remote(src, src, R.a2_s.at[k], R.a2_r.at[k], dev)
+        half = z // 2
+        for zs in (pl.ds(4 * half + 1 - z, 1), pl.ds(2 * (1 - half), 2)):
+            src = R.tok.at[zs, y, x, :, cds(k)]
+            remote(src, src, R.a2_s.at[k], R.a2_r.at[k], dev).start()
+        all3 = R.tok.at[pl.ds(0, 3), y, x, :, cds(k)]
+        return go(remote(all3, all3, R.a2_s.at[k], R.a2_r.at[k], dev), False)
+
+    def third_own(color, piece):
+        first, size = spans[color]
+        at = pl.ds(first + piece * (size // 2), size // 2)
+        if color:
+            src, dev = R.tok.at[z, :, x, :, at], to(x=1 - x)
+        else:
+            src, dev = R.tok.at[z, y, :, :, at], to(y=1 - y)
+        return remote(src, src, R.at_s.at[color, piece], R.at_r.at[color, piece], dev)
 
     def third(k):
-        if k < G:
-            src, dev = R.tok.at[:, y, :, :, cds(k)], to(y=1 - y)
-        else:
-            src, dev = R.tok.at[:, :, x, :, cds(k)], to(x=1 - x)
-        return remote(src, src, R.a3_s.at[k], R.a3_r.at[k], dev)
+        half = z // 2
+
+        def shards(zs):
+            if k < G:
+                return R.tok.at[zs, y, :, :, cds(k)]
+            return R.tok.at[zs, :, x, :, cds(k)]
+
+        dev = to(y=1 - y) if k < G else to(x=1 - x)
+        for zs in (pl.ds(4 * half + 1 - z, 1), pl.ds(2 * (1 - half), 2)):
+            remote(shards(zs), shards(zs), R.a3_s.at[k], R.a3_r.at[k], dev).start()
+        all3 = shards(pl.ds(0, 3))
+        return go(remote(all3, all3, R.a3_s.at[k], R.a3_r.at[k], dev), False)
 
     def up(t, first):
         tall = g.y * g.x * H
@@ -947,34 +1018,50 @@
             R.acc[at, :] = value if first else R.acc[at, :] + value
             return 0
 
-        lax.fori_loop(0, g.z, body, 0)
+        lax.fori_loop(0, g.z, body, 0, unroll=True)
 
     for t in range(G):
         for k in pair(t):
             ag[k].start()
-    own_weights(("down",))
-    pass_weights(NEAR + STRAIGHT, ("up",))
+    own_weights(1)
+    pass_weights(NEAR + STRAIGHT, 0)
+    own_second = [go(second_own(color)) for color in range(2)]
+    own_third = []
     flying = {}
-    for t in range(G + 2):
+    for t in range(G + 3):
         if t < G:
             for k in pair(t):
                 ag[k].forward()
             if t == G - 1:
-                relay_weights([1, 3, 2], ("up",))
-                send_weights(STRAIGHT, ("down",))
-                relay_weights([1, 3, 2], ("down",))
+                relay_weights([3, 2], 0)
+        if t in (1, 2):
+            for color in (1, 0):
+                if t == 1:
+                    own_second[color].wait_recv()
+                own_third.append(go(third_own(color, t - 1)))
         if 0 <= t - 1 < G:
             for k in pair(t - 1):
                 ag[k].finish()
-                flying[2, k] = go(second(k))
-        if 0 <= t - 2 < G:
-            for k in pair(t - 2):
+                flying[2, k] = second(k)
+        if t == LEND:
+            lend_weights([1, 3, 2], 1)
+            send_weights([(0, 1)], 1)
+        if 0 <= t - 3 < G:
+            for k in pair(t - 3):
                 flying[2, k].wait_recv()
-                flying[3, k] = go(third(k))
-    pass_weights(CROSS, ("up",))
+                flying[3, k] = third(k)
+        if t == G:
+            send_weights(STRAIGHT, 1)
+        if t == G + 1:
+            relay_weights([1, 3, 2], 1)
+    pass_weights(CROSS, 0)
     for p in range(Q):
         wait_weights(p, 0)
     for t in range(G):
+        if t == G - 1:
+            pass_weights(NEAR + STRAIGHT, 1)
+        for cp in own_third if t == 0 else ():
+            cp.wait_recv()
         for k in pair(t):
             flying[3, k].wait_recv()
         up(t, t == 0)
@@ -987,7 +1074,7 @@
     edges = go(
         remote(R.ed, R.er.at[:, pl.ds(8, 2 * Q), :], R.ed_s.at[0], R.ed_r.at[0], to(c=1 - c))
     )
-    pass_weights(NEAR + STRAIGHT + CROSS, ("down",))
+    pass_weights(CROSS, 1)
     edges.wait_recv()
     top = lax.broadcasted_iota(jnp.int32, (L, LANES), 0)
 
@@ -1011,7 +1098,7 @@
             ).astype(BF16)
         return 0
 
-    lax.fori_loop(0, Q, conv, 0)
+    lax.fori_loop(0, Q, conv, 0, unroll=2)
     for p in range(Q):
         wait_weights(p, 1)
 
@@ -1032,11 +1119,11 @@
 
         def body(i, _):
             at = pl.ds(pl.multiple_of(i * tall, tall), tall)
-            value = dot(R.hid[at, :], R.wdn[:, cols(k)], ((1,), (0,)))
-            R.part[i, :, :, :, cols(k)] = value.astype(BF16).reshape(g.y, g.x, H, f.reduce[k][1])
+            value = dot(R.hid[at, :], R.wdn[:, k], ((1,), (0,)))
+            R.part[i, :, :, :, k] = value.astype(BF16).reshape(g.y, g.x, H, k.stop - k.start)
             return 0
 
-        lax.fori_loop(0, g.z, body, 0)
+        lax.fori_loop(0, g.z, body, 0, unroll=True)
 
     def first_sum(k):
         if k < G:
@@ -1071,14 +1158,12 @@
         lax.fori_loop(0, g.z, body, 0)
 
     def last_sums(k):
-        sums = []
         for j in range(1, 4):
             zt = lax.rem(z + j, 4)
             src = R.part.at[zt, y, x, :, cds(k)]
-            sums.append(
-                go(remote(src, R.r3.at[j - 1, :, cds(k)], R.r3_s.at[k, j - 1], R.r3_r.at[k, j - 1], to(z=zt)))
-            )
-        return sums
+            remote(src, R.r3.at[j - 1, :, cds(k)], R.r3_s.at[k], R.r3_r.at[k], to(z=zt)).start()
+        all3 = R.r3.at[:, :, cds(k)]
+        return go(remote(all3, all3, R.r3_s.at[k], R.r3_r.at[k], to(y=1 - y)), False)
 
     def stage1(t):
         for k in pair(t):
@@ -1099,25 +1184,83 @@
     def stage4(t):
         for k in pair(t):
             total = R.after[:, cols(k)] + R.part[z, y, x, :, cols(k)].astype(F32)
-            for j, cp in enumerate(flying[6, k]):
-                cp.wait_recv()
+            flying[6, k].wait_recv()
+            for j in range(3):
                 total += R.r3[j, :, cols(k)].astype(F32)
             R.out[:, cols(k)] = total.astype(BF16)
 
+    V = f.side
+    both = slice(D - 2 * V, D)
+    one, two = slice(D - 2 * V, D - V), slice(D - V, D)
+
+    def ds(at):
+        return pl.ds(at.start, at.stop - at.start)
+
+    side = {}
+
+    def side1():
+        for j in range(1, 4):
+            zt = lax.rem(z + j, 4)
+            src = R.part.at[zt, :, :, :, ds(both)]
+            remote(src, R.c1.at[j - 1], R.c1_s.at[0], R.c1_r.at[0], to(z=zt)).start()
+        side[1] = go(remote(R.c1, R.c1, R.c1_s.at[0], R.c1_r.at[0], to(y=1 - y)), False)
+
+    def side2():
+        side[1].wait_recv()
+        for i in range(2 * g.y):
+            at = (z, i // 2, i % 2, slice(None), both)
+            total = R.part[at].astype(F32)
+            for j in range(3):
+                total += R.c1[j, i // 2, i % 2].astype(F32)
+            R.part[at] = total.astype(BF16)
+        src = R.part.at[z, :, 1 - x, :, ds(one)]
+        side[2, 0] = go(remote(src, R.c2.at[0], R.c2_s.at[0], R.c2_r.at[0], to(x=1 - x)))
+        src = R.part.at[z, 1 - y, :, :, ds(two)]
+        side[2, 1] = go(remote(src, R.c2.at[1], R.c2_s.at[1], R.c2_r.at[1], to(y=1 - y)))
+
+    def side3():
+        side[2, 0].wait_recv()
+        for i in range(2):
+            at = (z, i, x, slice(None), one)
+            R.part[at] = (R.part[at].astype(F32) + R.c2[0, i].astype(F32)).astype(BF16)
+        src = R.part.at[z, 1 - y, x, :, ds(one)]
+        side[3, 0] = go(remote(src, R.c3.at[0], R.c3_s.at[0], R.c3_r.at[0], to(y=1 - y)))
+        side[2, 1].wait_recv()
+        for i in range(2):
+            at = (z, y, i, slice(None), two)
+            R.part[at] = (R.part[at].astype(F32) + R.c2[1, i].astype(F32)).astype(BF16)
+        src = R.part.at[z, y, 1 - x, :, ds(two)]
+        side[3, 1] = go(remote(src, R.c3.at[1], R.c3_s.at[1], R.c3_r.at[1], to(x=1 - x)))
+
+    def side4():
+        for i, at in enumerate((one, two)):
+            side[3, i].wait_recv()
+            total = R.after[:, at] + R.part[z, y, x, :, at].astype(F32) + R.c3[i].astype(F32)
+            R.out[:, at] = total.astype(BF16)
+
     for t in range(G):
         for k in pair(t):
-            down(k)
+            down(cols(k))
             if t < 2:
                 flying[4, k] = go(first_sum(k))
+        if t == 0:
+            down(both)
+            side1()
     for t in range(G + 2):
         if t < G:
             stage2(t)
         if t + 2 < G:
             stage1(t + 2)
+        if t == 1:
+            side2()
         if 0 <= t - 1 < G:
             stage3(t - 1)
+        if t == 3:
+            side3()
         if 0 <= t - 2 < G:
             stage4(t - 2)
+        if t == G:
+            side4()
     for cond, cp in drains:
         if cond is None:
             cp.wait_send()
@@ -1132,7 +1275,7 @@
     return pl.pallas_call(
         functools.partial(fused_kernel, f, list(scratch)),
         out_shape=jax.ShapeDtypeStruct((f.rows, f.depth), BF16),
-        in_specs=[vmem] * 12 + [anyw] * 4,
+        in_specs=[anyw] * 5 + [vmem] * 3 + [anyw] + [vmem] * 3 + [anyw] * 4,
         out_specs=vmem,
         scratch_shapes=list(scratch.values()),
         compiler_params=pltpu.CompilerParams(
@@ -1178,7 +1321,7 @@
                 query_logits,
                 output_gate_logits,
                 forget_minimum,
-                extra_log_rate,
+                extra_log_rate.transpose(0, 2, 1),
                 head_norm_scale[None],
                 residual,
                 prenorm_scale[None],

time: 150 us -> 133 us (0.89)
  Pallas kernels: 147 us -> 131 us
    pallas_call x1, Pallas kernels: 147 us -> 131 us  [fused(): pl.pallas_call(functools.partial(fused_kernel, f, list(scratch)), out_sha...]
    unnamed x2 -> x1, local copies, waits for them, and re-layouts: 3.15 us -> 1.67 us
where the time goes in v3:
time: 133 us
  Pallas kernels  131 us (98%)
  local copies, waits for them, and re-layouts  1.67 us (1%)
    pallas_call x1, Pallas kernels, fused(): pl.pallas_call(functools.partial(fused_kernel, f, list(scratch)), out_sha...  131 us

profile of v3, /device:TPU:0, one launch (start us, length us, event | category | flops | bytes accessed | tf_op | source)
XLA Modules:
  0.0 133.1 jit_solution(13058137014157140329)
XLA Ops:
  0.0 131.4 %shard_map.154 = bf16[64,2048]{1,0:T(8,128)(2,1)} custom-call(bf16[128,512]{1,0:T(8,128)(2,1)} %refs_0_.1, bf16[128,512]{1,0:T(8,128)(2,1)} %refs_1_.1, bf16[128,512]{1,0:T(8,128)(2,1)} %refs_2_.1, bf16[128,512]{1,0:T(8,128)(2,1)} %refs_3_.1, bf16[128,512]{1,0:T(8,128)(2,1)} %refs_4_.1, f32[2,512]{1,0:T(2,128)} %refs_5_.1, f32[2,4,128]{2,1,0:T(4,128)} %bitcast.4, ...), custom_call_target="tpu_custom_call" | custom-call | tf_op jit(solution)/shard_map/pallas_call | solution.py:1275
  131.4 1.7 %copy.18 = bf16[64,2048]{1,0:T(8,128)(2,1)} copy(bf16[64,2048]{1,0:T(8,128)(2,1)} %shard_map.154) | data formatting | bytes 524288

commit v4 on v3

--- a/solution.py
+++ b/solution.py
@@ -479,7 +479,7 @@
             res=pltpu.VMEM((self.rows, self.depth), BF16),
             in_s=dma((6,)),
             loc_s=dma((1,)),
-            oz_s=dma((OUT_PIECES, 4)), oz_r=dma((OUT_PIECES, 4)),
+            oz_s=dma((OUT_PIECES, 2)), oz_r=dma((OUT_PIECES, 2)),
             oy_s=dma((OUT_PIECES,)), oy_r=dma((OUT_PIECES,)),
             oc_s=dma((OUT_PIECES,)), oc_r=dma((OUT_PIECES,)),
             xs_s=dma((4,)), xs_r=dma((4,)),
@@ -487,10 +487,10 @@
             sd=pltpu.VMEM((g.z - 1, self.unit, LANES), BF16),
             sy_s=dma((g.z - 1, 2)), sy_r=dma((g.z - 1, 2)),
             w_s=dma((self.quads, 2)), w_r=dma((self.quads, 2)),
-            f_s=dma((self.quads, 2)), f_r=dma((self.quads, 2)),
+            f_s=dma((2,)), f_r=dma((2,)),
             st_s=dma((4,)), st_r=dma((4,)),
             sz_s=dma((1,)), sz_r=dma((1,)),
-            az_s=dma((n, 4)), az_r=dma((n, 4)),
+            az_s=dma((n, 2)), az_r=dma((n, 2)),
             ao_s=dma((2,)), ao_r=dma((2,)),
             at_s=dma((2, 2)), at_r=dma((2, 2)),
             a2_s=dma((n,)), a2_r=dma((n,)),
@@ -666,12 +666,12 @@
             p = kin(dz, dy, -1)
             ref = spots(p * 2 + c, None)[kind]
             arrived(ref, kind, has_extra, R.w_r.at[p, kind])
-            go(remote(ref, ref, R.f_s.at[p, kind], R.f_r.at[p, kind], to(c=1 - c)))
-
-    def wait_weights(p, kind):
-        k = pl.ds(pl.multiple_of((p * 2 + 1 - c) * LANES, LANES), LANES)
-        ref = R.wup.at[k, :] if kind == 0 else R.wdn.at[:, k]
-        remote(ref, ref, R.f_s.at[p, kind], R.f_r.at[p, kind], to(c=1 - c)).wait_recv()
+            remote(ref, ref, R.f_s.at[kind], R.f_r.at[kind], to(c=1 - c)).start()
+
+    def wait_weights(kind):
+        count = pl.ds(0, Q * LANES)
+        ref = R.wdn.at[:, count] if kind else R.wup.at[count, :]
+        go(remote(ref, ref, R.f_s.at[kind], R.f_r.at[kind], to(c=1 - c)), False).wait_recv()
 
     mid = (z == 1) | (z == 2)
     t0, t1 = jnp.where(z == 1, 0, 1), jnp.where(z == 2, 3, 2)
@@ -680,37 +680,27 @@
     class ZGather:
         def __init__(self, src, dst, ss, rs):
             self.src, self.dst, self.ss, self.rs = src, dst, ss, rs
+            self.pair = dst(pl.ds(2 * (1 - z // 2), 2))
+            self.far = remote(self.pair, self.pair, ss(1), rs(1), to(z=far))
 
         def start(self):
-            for j, t in enumerate((t0, t1)):
-                go(remote(self.src, self.dst(z), self.ss(j), self.rs(z), to(z=t)))
-
-        def arrive(self, shard):
-            d = self.dst(shard)
-            remote(d, d, self.ss(0), self.rs(shard), to(z=t0)).wait_recv()
+            for t in (t0, t1):
+                slot = jnp.where(t // 2 == z // 2, 0, 1)
+                remote(self.src, self.dst(z), self.ss(0), self.rs(slot), to(z=t)).start()
+            go(remote(self.pair, self.pair, self.ss(0), self.rs(1), to(z=t0)), False)
 
         def forward(self):
-            for k in range(2):
-                shard = jnp.where(z == 1, 2 + k, k)
-                d = self.dst(shard)
-                cp = remote(d, d, self.ss(2 + k), self.rs(shard), to(z=far))
-
-                @pl.when(mid)
-                def _(cp=cp):
-                    cp.wait_recv()
-                    cp.start()
-
-                drains.append((mid, cp))
-
-        def finish(self):
             @pl.when(mid)
             def _():
-                self.arrive(far)
-
-            @pl.when(jnp.logical_not(mid))
-            def _():
-                for k in range(3):
-                    self.arrive(jnp.where(z == 0, 1 + k, k))
+                self.far.wait_recv()
+                self.far.start()
+
+            drains.append((mid, self.far))
+
+        def finish(self):
+            one = self.dst(z)
+            remote(one, one, self.ss(0), self.rs(0), to(z=t0)).wait_recv()
+            pl.when(jnp.logical_not(mid))(self.far.wait_recv)
 
     loads = [
         pltpu.make_async_copy(src, dst, R.in_s.at[i])
@@ -985,7 +975,8 @@
 
     def third_own(color, piece):
         first, size = spans[color]
-        at = pl.ds(first + piece * (size // 2), size // 2)
+        less = size // (2 * LANES) * LANES
+        at = pl.ds(first + piece * less, size - less if piece else less)
         if color:
             src, dev = R.tok.at[z, :, x, :, at], to(x=1 - x)
         else:
@@ -1032,7 +1023,7 @@
         if t < G:
             for k in pair(t):
                 ag[k].forward()
-            if t == G - 1:
+            if t == G - 2:
                 relay_weights([3, 2], 0)
         if t in (1, 2):
             for color in (1, 0):
@@ -1050,13 +1041,12 @@
             for k in pair(t - 3):
                 flying[2, k].wait_recv()
                 flying[3, k] = third(k)
+        if t == G - 1:
+            send_weights(STRAIGHT, 1)
         if t == G:
-            send_weights(STRAIGHT, 1)
-        if t == G + 1:
             relay_weights([1, 3, 2], 1)
     pass_weights(CROSS, 0)
-    for p in range(Q):
-        wait_weights(p, 0)
+    wait_weights(0)
     for t in range(G):
         if t == G - 1:
             pass_weights(NEAR + STRAIGHT, 1)
@@ -1098,9 +1088,8 @@
             ).astype(BF16)
         return 0
 
-    lax.fori_loop(0, Q, conv, 0, unroll=2)
-    for p in range(Q):
-        wait_weights(p, 1)
+    lax.fori_loop(0, Q, conv, 0, unroll=True)
+    wait_weights(1)
 
     n = len(f.reduce)
     G = n // 2

time: 133 us -> 132 us (level)
  no operation moved by 1% of the time
where the time goes in v4:
time: 132 us
  Pallas kernels  130 us (98%)
  local copies, waits for them, and re-layouts  1.67 us (1%)
    pallas_call x1, Pallas kernels, fused(): pl.pallas_call(functools.partial(fused_kernel, f, list(scratch)), out_sha...  130 us

profile of v4, /device:TPU:0, one launch (start us, length us, event | category | flops | bytes accessed | tf_op | source)
XLA Modules:
  0.0 131.8 jit_solution(12896612036209579501)
XLA Ops:
  0.0 130.1 %shard_map.154 = bf16[64,2048]{1,0:T(8,128)(2,1)} custom-call(bf16[128,512]{1,0:T(8,128)(2,1)} %refs_0_.1, bf16[128,512]{1,0:T(8,128)(2,1)} %refs_1_.1, bf16[128,512]{1,0:T(8,128)(2,1)} %refs_2_.1, bf16[128,512]{1,0:T(8,128)(2,1)} %refs_3_.1, bf16[128,512]{1,0:T(8,128)(2,1)} %refs_4_.1, f32[2,512]{1,0:T(2,128)} %refs_5_.1, f32[2,4,128]{2,1,0:T(4,128)} %bitcast.4, ...), custom_call_target="tpu_custom_call" | custom-call | tf_op jit(solution)/shard_map/pallas_call | solution.py:1264
  130.1 1.7 %copy.18 = bf16[64,2048]{1,0:T(8,128)(2,1)} copy(bf16[64,2048]{1,0:T(8,128)(2,1)} %shard_map.154) | data formatting | bytes 524288

commit v5 on v4

--- a/solution.py
+++ b/solution.py
@@ -384,7 +384,7 @@
 LANES = 128
 PAD_ROWS = 16
 GATHER_WIDTHS = ((1, 1, 2, 1, 1), (1, 2, 3, 2, 2))
-REDUCE_WIDTHS = ((1, 2, 2, 1, 1), (1, 2, 2, 1, 1))
+REDUCE_WIDTHS = ((2, 2, 2, 1), (2, 2, 2, 1))
 SIDE = 1
 LEND = 2
 OUT_PIECES = 4
@@ -468,6 +468,8 @@
             c1=pltpu.VMEM((g.z - 1, g.y, g.x, self.rows, 2 * self.side), BF16),
             c2=pltpu.VMEM((2, 2, self.rows, self.side), BF16),
             c3=pltpu.VMEM((2, self.rows, self.side), BF16),
+            o1_s=dma((2, 2)), o1_r=dma((2, 2)),
+            o2_s=dma((2, 2)), o2_r=dma((2, 2)),
             c1_s=dma((1,)), c1_r=dma((1,)),
             c2_s=dma((2,)), c2_r=dma((2,)),
             c3_s=dma((2,)), c3_r=dma((2,)),
@@ -1114,37 +1116,91 @@
 
         lax.fori_loop(0, g.z, body, 0, unroll=True)
 
+    half = z // 2
+    others = (pl.ds(4 * half + 1 - z, 1), pl.ds(2 * (1 - half), 2))
+
+    def ds(at):
+        return pl.ds(at.start, at.stop - at.start)
+
+    def first_part(zs, color, at):
+        if color == 0:
+            return R.part.at[zs, 1 - y, :, :, at], to(y=1 - y)
+        return R.part.at[zs, :, 1 - x, :, at], to(x=1 - x)
+
+    def second_part(zs, color, at):
+        if color == 0:
+            return R.part.at[zs, y, 1 - x, :, at], to(x=1 - x)
+        return R.part.at[zs, 1 - y, x, :, at], to(y=1 - y)
+
     def first_sum(k):
-        if k < G:
-            src, dev = R.part.at[:, 1 - y, :, :, cds(k)], to(y=1 - y)
-        else:
-            src, dev = R.part.at[:, :, 1 - x, :, cds(k)], to(x=1 - x)
-        return remote(src, R.r1.at[:, :, :, cds(k)], R.r1_s.at[k], R.r1_r.at[k], dev)
+        for zs in others:
+            src, dev = first_part(zs, k // G, cds(k))
+            remote(src, R.r1.at[zs, :, :, cds(k)], R.r1_s.at[k], R.r1_r.at[k], dev).start()
+        all3 = R.r1.at[pl.ds(0, 3), :, :, cds(k)]
+        return go(remote(all3, all3, R.r1_s.at[k], R.r1_r.at[k], dev), False)
 
     def second_sum(k):
-        if k < G:
-            src, dev = R.part.at[:, y, 1 - x, :, cds(k)], to(x=1 - x)
-        else:
-            src, dev = R.part.at[:, 1 - y, x, :, cds(k)], to(y=1 - y)
-        return remote(src, R.r2.at[:, :, cds(k)], R.r2_s.at[k], R.r2_r.at[k], dev)
+        for zs in others:
+            src, dev = second_part(zs, k // G, cds(k))
+            remote(src, R.r2.at[zs, :, cds(k)], R.r2_s.at[k], R.r2_r.at[k], dev).start()
+        all3 = R.r2.at[pl.ds(0, 3), :, cds(k)]
+        return go(remote(all3, all3, R.r2_s.at[k], R.r2_r.at[k], dev), False)
+
+    def add_one(zi, j, color, at):
+        where = ((zi, y, j) if color == 0 else (zi, j, x)) + (slice(None), at)
+        R.part[where] = (R.part[where].astype(F32) + R.r1[zi, j, :, at].astype(F32)).astype(BF16)
 
     def add_first(k):
         def body(i, _):
-            zi, j = i // 2, lax.rem(i, 2)
-            at = (zi, y, j) if k < G else (zi, j, x)
-            at = at + (slice(None), cols(k))
-            R.part[at] = (R.part[at].astype(F32) + R.r1[zi, j, :, cols(k)].astype(F32)).astype(BF16)
+            add_one(lax.rem(z + 1 + i // 2, 4), lax.rem(i, 2), k // G, cols(k))
             return 0
 
-        lax.fori_loop(0, 2 * g.z, body, 0)
+        lax.fori_loop(0, 2 * (g.z - 1), body, 0)
 
     def add_second(k):
         def body(i, _):
-            at = (i, y, x, slice(None), cols(k))
-            R.part[at] = (R.part[at].astype(F32) + R.r2[i, :, cols(k)].astype(F32)).astype(BF16)
+            zi = lax.rem(z + 1 + i, 4)
+            at = (zi, y, x, slice(None), cols(k))
+            R.part[at] = (R.part[at].astype(F32) + R.r2[zi, :, cols(k)].astype(F32)).astype(BF16)
             return 0
 
-        lax.fori_loop(0, g.z, body, 0)
+        lax.fori_loop(0, g.z - 1, body, 0)
+
+    ends = (0, f.reduce[G][0], D - 2 * f.side)
+    mine_sums = {}
+
+    def own_span(color, piece):
+        first, size = ends[color], ends[color + 1] - ends[color]
+        less = -(-size // (2 * LANES)) * LANES
+        return slice(first + less, first + size) if piece else slice(first, first + less)
+
+    def own_first(piece):
+        for color in range(2):
+            at = ds(own_span(color, piece))
+            src, dev = first_part(z, color, at)
+            dst = R.r1.at[z, :, :, at]
+            sems = R.o1_s.at[color, piece], R.o1_r.at[color, piece]
+            mine_sums[1, color, piece] = go(remote(src, dst, *sems, dev))
+
+    def own_next(piece):
+        for color in range(2):
+            span = own_span(color, piece)
+            mine_sums[1, color, piece].wait_recv()
+            for j in range(2):
+                add_one(z, j, color, span)
+            src, dev = second_part(z, color, ds(span))
+            dst = R.r2.at[z, :, ds(span)]
+            sems = R.o2_s.at[color, piece], R.o2_r.at[color, piece]
+            mine_sums[2, color, piece] = go(remote(src, dst, *sems, dev))
+
+    def own_last(piece):
+        for color in range(2):
+            at = own_span(color, piece)
+            mine_sums[2, color, piece].wait_recv()
+            total = R.after[:, at] + R.part[z, y, x, :, at].astype(F32) + R.r2[z, :, at].astype(F32)
+            for j in range(3):
+                total += R.r3[j, :, at].astype(F32)
+            R.out[:, at] = total.astype(BF16)
 
     def last_sums(k):
         for j in range(1, 4):
@@ -1156,13 +1212,13 @@
 
     def stage1(t):
         for k in pair(t):
-            flying[4, k] = go(first_sum(k))
+            flying[4, k] = first_sum(k)
 
     def stage2(t):
         for k in pair(t):
             flying[4, k].wait_recv()
             add_first(k)
-            flying[5, k] = go(second_sum(k))
+            flying[5, k] = second_sum(k)
 
     def stage3(t):
         for k in pair(t):
@@ -1170,20 +1226,9 @@
             add_second(k)
             flying[6, k] = last_sums(k)
 
-    def stage4(t):
-        for k in pair(t):
-            total = R.after[:, cols(k)] + R.part[z, y, x, :, cols(k)].astype(F32)
-            flying[6, k].wait_recv()
-            for j in range(3):
-                total += R.r3[j, :, cols(k)].astype(F32)
-            R.out[:, cols(k)] = total.astype(BF16)
-
     V = f.side
     both = slice(D - 2 * V, D)
     one, two = slice(D - 2 * V, D - V), slice(D - V, D)
-
-    def ds(at):
-        return pl.ds(at.start, at.stop - at.start)
 
     side = {}
 
@@ -1231,25 +1276,33 @@
         for k in pair(t):
             down(cols(k))
             if t < 2:
-                flying[4, k] = go(first_sum(k))
+                flying[4, k] = first_sum(k)
         if t == 0:
             down(both)
             side1()
-    for t in range(G + 2):
+    for t in range(G + 1):
         if t < G:
             stage2(t)
         if t + 2 < G:
             stage1(t + 2)
+        if t == G - 2:
+            own_first(0)
+        if t == G - 1:
+            own_first(1)
         if t == 1:
             side2()
         if 0 <= t - 1 < G:
             stage3(t - 1)
         if t == 3:
             side3()
-        if 0 <= t - 2 < G:
-            stage4(t - 2)
-        if t == G:
-            side4()
+    own_next(0)
+    own_next(1)
+    side4()
+    for t in range(G):
+        for k in pair(t):
+            flying[6, k].wait_recv()
+    own_last(0)
+    own_last(1)
     for cond, cp in drains:
         if cond is None:
             cp.wait_send()

time: 132 us -> 128 us (0.970)
  Pallas kernels: 130 us -> 126 us
    pallas_call x1, Pallas kernels: 130 us -> 126 us  [fused(): pl.pallas_call(functools.partial(fused_kernel, f, list(scratch)), out_sha...]
where the time goes in v5:
time: 128 us
  Pallas kernels  126 us (98%)
  local copies, waits for them, and re-layouts  1.67 us (1%)
    pallas_call x1, Pallas kernels, fused(): pl.pallas_call(functools.partial(fused_kernel, f, list(scratch)), out_sha...  126 us

profile of v5, /device:TPU:0, one launch (start us, length us, event | category | flops | bytes accessed | tf_op | source)
XLA Modules:
  0.0 127.8 jit_solution(9010364558425732928)
XLA Ops:
  0.0 126.1 %shard_map.154 = bf16[64,2048]{1,0:T(8,128)(2,1)} custom-call(bf16[128,512]{1,0:T(8,128)(2,1)} %refs_0_.1, bf16[128,512]{1,0:T(8,128)(2,1)} %refs_1_.1, bf16[128,512]{1,0:T(8,128)(2,1)} %refs_2_.1, bf16[128,512]{1,0:T(8,128)(2,1)} %refs_3_.1, bf16[128,512]{1,0:T(8,128)(2,1)} %refs_4_.1, f32[2,512]{1,0:T(2,128)} %refs_5_.1, f32[2,4,128]{2,1,0:T(4,128)} %bitcast.4, ...), custom_call_target="tpu_custom_call" | custom-call | tf_op jit(solution)/shard_map/pallas_call | solution.py:1317
  126.1 1.7 %copy.18 = bf16[64,2048]{1,0:T(8,128)(2,1)} copy(bf16[64,2048]{1,0:T(8,128)(2,1)} %shard_map.154) | data formatting | bytes 524288
